TPU v7x, 256 devices: a whole 4x4x8 slice. The times are simulated.
256 devices in a mesh: sp: 64 (over z, y, core), tp: 4 (over x).
Axes of the slice: x: 4, y: 4, z: 8, core: 2. Of those that a mesh axis runs over, the one named last changes fastest.
Arguments:
- tokens: bfloat16 [10240, 2048], P('sp'), may hold values from -8 to 8
- query_weight: bfloat16 [2048, 2048], P('sp', 'tp'), may hold values from -0.5 to 0.5
- key_weight: bfloat16 [2048, 2048], P('sp', 'tp'), may hold values from -0.5 to 0.5
- value_weight: bfloat16 [2048, 2048], P('sp', 'tp'), may hold values from -0.125 to 0.125
- out_weight: bfloat16 [2048, 2048], P('tp', 'sp'), may hold values from -0.125 to 0.125
- mix_lambda: float32 [16], P('tp'), may hold values from 0.3 to 0.8
- head_gain: float32 [128], replicated, may hold values from 0.1 to 1.9
Outputs:
- attended: bfloat16 [10240, 2048], P('sp')
All inputs are finite; a program needn't handle non-finite values.
Results may differ from a plain program's by a relative error of at most 0.018.
The roundings to bfloat16 on the way count: a program that leaves them out, or rounds other values in their place, can miss the bound.
Values may be sent and summed in bfloat16 or wider, within the bound.
A program may use at most 192 MiB of HBM per device.

v0:
```python
import jax
import jax.numpy as jnp
from jax import lax
from jax.sharding import PartitionSpec as P


def gather_turned(arrays, axis, dims):
    turned = [jnp.moveaxis(a, dim, 0) for a, dim in zip(arrays, dims)]
    widths = [t[0].size for t in turned]
    both = jnp.concatenate([t.reshape(-1, w) for t, w in zip(turned, widths)], axis=1)
    out = lax.all_gather(both, axis, axis=0, tiled=True)
    parts = jnp.split(out, [sum(widths[:k]) for k in range(1, len(widths))], axis=1)
    return tuple(
        (
            jnp.moveaxis(b.reshape(-1, *t.shape[1:]), 0, dim)
            for b, t, dim in zip(parts, turned, dims)
        )
    )


def sent_together(arrays, axis, dim, along):
    columns = [a.reshape(*a.shape[:along], -1) for a in arrays]
    both = jnp.concatenate(columns, axis=along)
    out, at, gathered = (lax.all_gather(both, axis, axis=dim, tiled=True), 0, [])
    for a, column in zip(arrays, columns):
        slab = out[..., at : at + column.shape[along]]
        gathered.append(slab.reshape(*slab.shape[:along], *a.shape[along:]))
        at += column.shape[along]
    return tuple(gathered)


def filled_up(lines, devices):
    spare = -len(lines) % devices
    return jnp.pad(lines, [(0, spare)] + [(0, 0)] * (lines.ndim - 1))


def total_of(x, axis):
    lines = x.reshape(-1, *x.shape[1:][-1:])
    own = lax.psum_scatter(
        filled_up(lines, lax.axis_size(axis)), axis, scatter_dimension=0, tiled=True
    )
    whole = lax.all_gather(own, axis).reshape(-1, *lines.shape[1:])
    return lax.slice_in_dim(whole, 0, len(lines)).reshape(x.shape)


def attend(state, query_rows, query_pos, key_rows, value_rows):
    maxima, totals, accum = state
    score_scale = key_rows.shape[-1] ** (-0.5)
    scores = (
        jnp.einsum("qhcd,khcd->hcqk", query_rows, key_rows, preferred_element_type=jnp.float32)
        * score_scale
    )
    key_pos = jnp.arange(key_rows.shape[0], dtype=jnp.int32)
    visible = key_pos[None, :] <= query_pos[:, None]
    scores = jnp.where(visible, scores, -1e30)
    new_max = jnp.maximum(maxima, jnp.max(scores, axis=-1))
    weights = jnp.exp(scores - new_max[..., None])
    totals = jnp.sum(weights, axis=-1)
    accum = jnp.einsum(
        "hcqk,khd->hcqd",
        weights.astype(jnp.bfloat16),
        value_rows,
        preferred_element_type=jnp.float32,
    )
    return (new_max, totals, accum)


def finish(state, mix_lambda, head_gain):
    maxima, totals, accum = state
    mixture = accum[:, 0] / totals[:, 0, :, None] - mix_lambda[:, None, None] * (
        accum[:, 1] / totals[:, 1, :, None]
    )
    normalized = (
        mixture * lax.rsqrt(jnp.mean(mixture * mixture, axis=-1, keepdims=True) + 1e-05) * head_gain
    )
    return (
        jnp.transpose(normalized, (1, 0, 2)).reshape(normalized.shape[1], -1).astype(jnp.bfloat16)
    )


def on_device(tokens, query_weight, key_weight, value_weight, out_weight, mix_lambda, head_gain):
    seq_index = lax.axis_index("sp")
    query_full, key_full, value_full, out_full = gather_turned(
        (query_weight, key_weight, value_weight, out_weight), "sp", (0, 0, 0, 1)
    )
    queries = jnp.dot(tokens, query_full, preferred_element_type=jnp.float32).astype(jnp.bfloat16)
    keys = jnp.dot(tokens, key_full, preferred_element_type=jnp.float32).astype(jnp.bfloat16)
    values = jnp.dot(tokens, value_full, preferred_element_type=jnp.float32).astype(jnp.bfloat16)
    heads_here = mix_lambda.shape[0]
    value_width = head_gain.shape[0]
    qk_width = value_width // 2
    row_count = keys.shape[0]
    half_rows = row_count // 2
    keys = keys.reshape(row_count, heads_here, 2, qk_width)
    values = values.reshape(row_count, heads_here, value_width)
    seq_start = seq_index * row_count
    offsets = jnp.arange(half_rows, dtype=jnp.int32)
    first_half = queries[:half_rows]
    second_half = queries[half_rows:]
    first_pos = seq_start + offsets
    second_pos = seq_start + half_rows + offsets
    first_half = first_half.reshape(half_rows, heads_here, 2, qk_width)
    second_half = second_half.reshape(half_rows, heads_here, 2, qk_width)

    def visit(state, query_rows, query_pos, key_rows, value_rows, key_start):

        def update(inner):
            return attend(inner, query_rows, query_pos, key_rows, value_rows)

        def keep(inner):
            return inner

        return lax.cond(key_start <= query_pos[half_rows - 1], update, keep, state)

    start_state = (
        jnp.full((heads_here, 2, half_rows), -1e30, jnp.float32),
        jnp.zeros((heads_here, 2, half_rows), jnp.float32),
        jnp.zeros((heads_here, 2, half_rows, value_width), jnp.float32),
    )
    key_start = jnp.int32(0)
    key_rows, value_rows = sent_together((keys, values), "sp", 0, 2)
    first_state = visit(start_state, first_half, first_pos, key_rows, value_rows, key_start)
    second_state = visit(start_state, second_half, second_pos, key_rows, value_rows, key_start)
    first_out = finish(first_state, mix_lambda, head_gain)
    second_out = finish(second_state, mix_lambda, head_gain)
    head_out = jnp.concatenate([first_out, second_out], axis=0)
    partial_out = jnp.dot(head_out, out_full, preferred_element_type=jnp.float32)
    summed = total_of(partial_out.astype(jnp.bfloat16), "tp").astype(jnp.float32)
    return summed.astype(jnp.bfloat16)


def solution(mesh):
    placed = (
        P("sp", None),
        P("sp", "tp"),
        P("sp", "tp"),
        P("sp", "tp"),
        P("tp", "sp"),
        P("tp"),
        P(),
    )
    return jax.shard_map(
        on_device, mesh=mesh, in_specs=placed, out_specs=P("sp", None), check_vma=False
    )
```

profile of v0, /device:TPU:224, one launch (start us, length us, event | category | flops | bytes accessed | tf_op | source)
XLA Modules:
  0.0 380.0 jit_solution(17578282885183539984)
XLA Ops:
  6.5 0.0 copy-start
  6.5 0.0 all-gather.4.cloned.1.call-start
  6.5 1.5 pad_maximum_fusion.1
  8.1 0.0 all-gather.4.cloned.1.call-update
  8.1 0.0 all-gather.6.cloned.1.call-start
  8.2 84.0 %all-gather.4.cloned.1.call-done = bf16[2048,2048]{1,0:T(8,128)(2,1)} async-done(((bf16[32,2048]{1,0:T(8,128)(2,1)}), bf16[2048,2048]{1,0:T(8,128)(2,1)}) %all-gather.4.cloned.1.call-update) | async-done | bytes 8388624 | tf_op jit(solution)/shard_map/all_gather | solution.py:11
  92.1 0.0 copy-done
  92.1 2.1 fusion.40
  94.3 2.1 fusion.43
  96.4 0.9 pad_maximum_fusion
  97.3 0.0 all-gather.6.cloned.1.call-update
  97.3 0.0 reduce-scatter.2.cloned.1.call-start
  97.4 0.6 slice.44
  98.7 0.6 slice.51
  100.0 2.1 fusion.46
  102.1 101.7 %all-gather.6.cloned.1.call-done = bf16[10240,4,256]{2,1,0:T(4,128)(2,1)} async-done(((bf16[160,4,256]{2,1,0:T(4,128)(2,1)}), bf16[10240,4,256]{2,1,0:T(4,128)(2,1)}) %all-gather.6.cloned.1.call-update) | async-done | bytes 20971536 | tf_op jit(solution)/shard_map/all_gather | solution.py:24
  203.8 19.5 %fusion.64 = (bf16[10240,4,128]{2,1,0:T(4,128)(2,1)}, bf16[10240,4,128]{2,1,0:T(4,128)(2,1)}) fusion(bf16[10240,4,256]{2,1,0:T(4,128)(2,1)} %all-gather.6.cloned.1.call-done), kind=kLoop, calls=%fused_computation.73 | loop fusion | bytes 41943040 | tf_op jit(solution)/shard_map/slice | solution.py:26
  223.3 16.9 %copy.42 = bf16[10240,4,128]{0,2,1:T(8,128)(2,1)} copy(bf16[10240,4,128]{2,1,0:T(4,128)(2,1)} %get-tuple-element.74) | data formatting | bytes 20971520
  240.2 45.6 %conditional.2 = (f32[4,2,80]{2,1,0:T(2,128)S(1)}, f32[4,2,80,128]{3,2,1,0:T(8,128)S(1)}) conditional(s32[]{:T(128)} %bitcast.4, () %tuple.21, (s32[80]{0:T(128)S(1)}, bf16[160,512]{1,0:T(8,128)(2,1)S(1)}, bf16[10240,4,2,64]{0,3,2,1:T(8,128)(2,1)}, bf16[10240,4,128]{2,1,0:T(4,128)(2,1)}) %tuple.52), branch_computations={%region_0.0_spmd, %region_1.4_spmd} | conditional | flops 2589490688 | bytes 103808336 | solution.py:113
  240.2 0.1 copy.27
  240.3 0.5 iota_compare_fusion
  240.8 13.8 %fusion = (f32[4,2,80]{2,1,0:T(2,128)S(1)}, f32[4,2,80,10240]{3,2,1,0:T(8,128)}) fusion(pred[80,10240]{1,0:T(8,128)(4,1)S(1)} %iota_compare_fusion, bf16[80,4,2,64]{0,3,2,1:T(8,128)(2,1)S(1)} %bitcast.71, bf16[10240,4,2,64]{0,3,2,1:T(8,128)(2,1)} %get-tuple-element.27), kind=kOutput, calls=%fused_computation.2 | convolution fusion | flops 858520960 | bytes 37603840 | tf_op jit(solution)/shard_map/cond/branch_1_fun/qhcd,khcd->hcqk/dot_general | solution.py:50
  254.6 19.0 %fusion.3 = f32[4,2,80,128]{3,2,1,0:T(8,128)S(1)} fusion(f32[4,2,80,10240]{3,2,1,0:T(8,128)} %get-tuple-element.70, f32[4,2,80]{2,1,0:T(2,128)S(1)} %broadcast_maximum_fusion, pred[80,10240]{1,0:T(8,128)(4,1)S(1)} %iota_compare_fusion, bf16[10240,4,128,1]{2,1,0,3:T(4,128)(2,1)} %bitcast.69), kind=kOutput, calls=%fused_computation.5 | convolution fusion | flops 1703936000 | bytes 37849600 | tf_op jit(solution)/shard_map/cond/branch_1_fun/hcqk,khd->hcqd/dot_general | solution.py:59
  273.6 12.2 %fusion.2 = f32[4,2,80]{2,1,0:T(2,128)S(1)} fusion(f32[4,2,80,10240]{3,2,1,0:T(8,128)} %get-tuple-element.70, f32[4,2,80]{2,1,0:T(2,128)S(1)} %broadcast_maximum_fusion, pred[80,10240]{1,0:T(8,128)(4,1)S(1)} %iota_compare_fusion), kind=kLoop, calls=%fused_computation.4 | loop fusion | flops 26213760 | bytes 27038720 | tf_op jit(solution)/shard_map/cond/branch_1_fun/reduce_sum | solution.py:58
  285.8 0.0 copy-start.2
  285.8 0.0 copy-start.3
  285.8 45.9 %conditional.3 = (f32[4,2,80]{2,1,0:T(2,128)S(1)}, f32[4,2,80,128]{3,2,1,0:T(8,128)S(1)}) conditional(s32[]{:T(128)} %bitcast.15, () %tuple.23, (s32[80]{0:T(128)S(1)}, bf16[160,512]{1,0:T(8,128)(2,1)S(1)}, bf16[10240,4,2,64]{0,3,2,1:T(8,128)(2,1)}, bf16[10240,4,128]{2,1,0:T(4,128)(2,1)}) %tuple.53), branch_computations={%region_5.6_spmd, %region_6.9_spmd} | conditional | flops 2589490688 | bytes 103808336 | solution.py:113
  286.0 0.1 copy.32
  286.2 0.1 slice.57
  286.3 0.5 iota_compare_fusion.1
  286.8 13.8 %fusion.12 = (f32[4,2,80]{2,1,0:T(2,128)S(1)}, f32[4,2,80,10240]{3,2,1,0:T(8,128)}) fusion(pred[80,10240]{1,0:T(8,128)(4,1)S(1)} %iota_compare_fusion.1, bf16[80,4,2,64]{0,3,2,1:T(8,128)(2,1)S(1)} %bitcast.72, bf16[10240,4,2,64]{0,3,2,1:T(8,128)(2,1)} %get-tuple-element.31), kind=kOutput, calls=%fused_computation.17 | convolution fusion | flops 858520960 | bytes 37603840 | tf_op jit(solution)/shard_map/cond/branch_1_fun/qhcd,khcd->hcqk/dot_general | solution.py:50
  300.6 19.0 %fusion.15 = f32[4,2,80,128]{3,2,1,0:T(8,128)S(1)} fusion(f32[4,2,80,10240]{3,2,1,0:T(8,128)} %get-tuple-element.72, f32[4,2,80]{2,1,0:T(2,128)S(1)} %broadcast_maximum_fusion.1, pred[80,10240]{1,0:T(8,128)(4,1)S(1)} %iota_compare_fusion.1, bf16[10240,4,128,1]{2,1,0,3:T(4,128)(2,1)} %bitcast.70), kind=kOutput, calls=%fused_computation.20 | convolution fusion | flops 1703936000 | bytes 37849600 | tf_op jit(solution)/shard_map/cond/branch_1_fun/hcqk,khd->hcqd/dot_general | solution.py:59
  319.6 12.2 %fusion.14 = f32[4,2,80]{2,1,0:T(2,128)S(1)} fusion(f32[4,2,80,10240]{3,2,1,0:T(8,128)} %get-tuple-element.72, f32[4,2,80]{2,1,0:T(2,128)S(1)} %broadcast_maximum_fusion.1, pred[80,10240]{1,0:T(8,128)(4,1)S(1)} %iota_compare_fusion.1), kind=kLoop, calls=%fused_computation.19 | loop fusion | flops 26213760 | bytes 27038720 | tf_op jit(solution)/shard_map/cond/branch_1_fun/reduce_sum | solution.py:58
  331.8 0.0 copy-start.1
  331.8 0.0 copy-done.2
  331.8 0.4 multiply_reduce_fusion.1
  332.2 0.0 copy-done.3
  332.3 0.2 fusion.59
  332.5 3.3 convolution_convert_fusion
  335.7 0.0 reduce-scatter.2.cloned.1.call-update
  335.8 23.7 %reduce-scatter.2.cloned.1.call-done = bf16[40,2048]{1,0:T(8,128)(2,1)} async-done(((bf16[160,2048]{1,0:T(8,128)(2,1)}), bf16[40,2048]{1,0:T(8,128)(2,1)}) %reduce-scatter.2.cloned.1.call-update) | async-done | bytes 163856 | tf_op jit(solution)/shard_map/reduce_scatter | solution.py:39
  359.4 13.2 %all-gather = bf16[160,2048]{1,0:T(8,128)(2,1)S(1)} all-gather(bf16[40,2048]{1,0:T(8,128)(2,1)} %reduce-scatter.2.cloned.1.call-done), channel_id=2, replica_groups=mesh['sp'=64,'tp'=4] {'tp'}, dimensions={0}, use_global_device_ids=true | all-gather | bytes 819200 | tf_op jit(solution)/shard_map/all_gather | solution.py:42
  372.7 0.8 copy.66
  373.5 0.0 copy-done.1
  (12 shorter events, 0.2 us)
Async XLA Ops:
  6.5 85.6 %copy-start = (bf16[160,2048]{1,0:T(8,128)(2,1)S(1)}, bf16[160,2048]{1,0:T(8,128)(2,1)}, u32[]{:S(2)}) copy-start(bf16[160,2048]{1,0:T(8,128)(2,1)} %param.11) | copy-start | bytes 1966084
  6.5 85.6 %all-gather.4.cloned.1.call-start = ((), (), s32[]{:S(2)}) async-start(), calls=%async_computation.1 | async-start | bytes 8519680 | tf_op jit(solution)/shard_map/all_gather | solution.py:11
  8.1 195.7 %all-gather.6.cloned.1.call-start = ((), (), s32[]{:S(2)}) async-start(), calls=%async_computation.2 | async-start | bytes 21299200 | tf_op jit(solution)/shard_map/all_gather | solution.py:24
  97.3 262.1 %reduce-scatter.2.cloned.1.call-start = ((), (), s32[]{:S(2)}) async-start(), calls=%async_computation.3 | async-start | bytes 819200 | tf_op jit(solution)/shard_map/reduce_scatter | solution.py:39
  285.8 46.0 %copy-start.2 = (f32[4]{0:T(128)S(1)}, f32[4]{0:T(128)}, u32[]{:S(2)}) copy-start(f32[4]{0:T(128)} %param.16) | copy-start | bytes 52
  285.8 46.4 %copy-start.3 = (f32[128]{0:T(128)S(1)}, f32[128]{0:T(128)}, u32[]{:S(2)}) copy-start(f32[128]{0:T(128)} %param.17) | copy-start | bytes 1540
  331.8 41.8 %copy-start.1 = (bf16[160,2048]{1,0:T(8,128)(2,1)S(1)}, bf16[160,2048]{1,0:T(8,128)(2,1)}, u32[]{:S(2)}) copy-start(bf16[160,2048]{1,0:T(8,128)(2,1)} %param.11) | copy-start | bytes 1966084
Sparse Core Ops, SparseCore 0:
  10.1 81.9 all-gather.3
  97.5 106.3 all-gather.5
  335.9 23.4 reduce-scatter.1
where the time goes:
time: 383 us; the launch traced here: 380 us
  waiting for transfers between devices  209 us (55%)
  matrix products  75.1 us (20%)
  local copies, waits for them, and re-layouts  39 us (10%)
  other arithmetic  28.4 us (7%)
  between operations  14.6 us (4%)
  blocking collectives  13.2 us (3%)
    all_gather x1, waiting for transfers between devices, sent_together(): lax.all_gather(both, axis, axis=dim, tiled=True)  102 us
    all_gather x1, waiting for transfers between devices, gather_turned(): out = lax.all_gather(both, axis, axis=0, tiled=True)  84 us
    dot_general x2, matrix products, attend(): jnp.einsum('hcqk,khd->hcqd', weights.astype(jnp.bfloat16), value_rows, pr...  38 us
    dot_general x2, matrix products, attend(): jnp.einsum('qhcd,khcd->hcqk', query_rows, key_rows, preferred_element_typ...  27.5 us
    reduce_sum x2, other arithmetic, attend(): totals = jnp.sum(weights, axis=-1)  24.3 us
    reduce_scatter x1, waiting for transfers between devices, total_of(): lax.psum_scatter(filled_up(lines, lax.axis_size(axis)), axis, scatter_dim...  23.7 us
    slice x1, local copies, waits for them, and re-layouts, sent_together(): slab = out[..., at:at + column.shape[along]]  19.5 us
    unnamed x10, local copies, waits for them, and re-layouts  17.7 us
  transfers between devices with their start and end apart: 3, of which 3 were waited for; matrix products, arithmetic and copies ran while one was open for 1% of the time, Pallas kernels for 0%

commit v1 on v0

v1 whole, which is shorter than its diff:
```python
import functools
import math

import jax
import jax.numpy as jnp
from jax import lax
from jax.experimental import pallas as pl
from jax.experimental.pallas import tpu as pltpu
from jax.sharding import Mesh
from jax.sharding import PartitionSpec as P

MESH = pl.DeviceIdType.MESH
NZ, NY, NC, NX = 8, 4, 2, 4
ROWS = 160
TOKS = NY * ROWS
HEAD = 128
COLS = 2 * TOKS
TILE = 256
LOW = -1e30
EXP_SCALE = 64 ** (-0.5) * math.log2(math.e)


def rcopy(src, dst, send_sem, recv_sem, device):
    return pltpu.make_async_remote_copy(
        src_ref=src, dst_ref=dst, send_sem=send_sem, recv_sem=recv_sem, device_id=device, device_id_type=MESH
    )


class ZRing:
    def __init__(self, block, send, recv, sib_send):
        self.block, self.send, self.recv, self.sib_send = block, send, recv, sib_send
        self.z, self.c = lax.axis_index("z"), lax.axis_index("core")

    def origin(self, way, d):
        return lax.rem(self.z + (NZ - d if way == 0 else d), NZ)

    def farthest(self, way, kind):
        return NZ // 2 - (way != kind)

    def onward(self, way, d, kind, o):
        ref = self.block(o, self.c, kind)
        to = lax.rem(self.z + (1 if way == 0 else NZ - 1), NZ)
        return rcopy(ref, ref, self.send.at[way, d - 1, kind], self.recv.at[o, self.c, kind], {"z": to})

    def share(self, o, kind):
        ref = self.block(o, self.c, kind)
        return rcopy(ref, ref, self.sib_send.at[o, kind], self.recv.at[o, self.c, kind], {"core": 1 - self.c})

    def arrived(self, o, c, kind):
        ref = self.block(o, c, kind)
        rcopy(ref, ref, self.sib_send.at[o, kind], self.recv.at[o, c, kind], {"core": 1 - self.c}).wait_recv()

    def begin(self, kind):
        for way in (0, 1):
            self.onward(way, 1, kind, self.z).start()
        self.share(self.z, kind).start()

    def pass_on(self, way, d, kind):
        o = self.origin(way, d)
        self.arrived(o, self.c, kind)

        @pl.when(d < self.farthest(way, kind))
        def _():
            self.onward(way, d + 1, kind, o).start()

        self.share(o, kind).start()

    def drain(self):
        for kind in (0, 1):
            for way in (0, 1):
                for d in range(1, self.farthest(way, kind) + 1):
                    self.onward(way, d, kind, self.z).wait_send()

            @pl.loop(0, NZ)
            def _(o):
                self.share(o, kind).wait_send()


def attention_kernel(
    tok, wq, wk, wv, lam, gain, out,
    xbuf, wbuf, kbuf, vbuf, qrow, vrow, qbd, acc, top,
    tok_s, tok_r, wy_s, wy_r, w_s, w_r, w_sib, kv_s, kv_r, kv_sib,
):
    z, y, c = lax.axis_index("z"), lax.axis_index("y"), lax.axis_index("core")
    above, below = lax.rem(y + 1, NY), lax.rem(y + NY - 1, NY)
    across = lax.rem(y + 2, NY)

    barrier = pltpu.get_barrier_semaphore()
    friends = [{"y": lax.rem(y + k, NY)} for k in range(1, NY)]
    friends += [{"z": lax.rem(z + 1, NZ)}, {"z": lax.rem(z + NZ - 1, NZ)}, {"core": 1 - c}]
    for friend in friends:
        pl.semaphore_signal(barrier, inc=1, device_id=friend, device_id_type=MESH)
    pl.semaphore_wait(barrier, len(friends))

    half = ROWS // 2

    def part(slot, k):
        return xbuf.at[slot, pl.ds(k * half, half), :]

    def tok_copy(src, slot, k, n, to):
        return rcopy(src, part(slot, k), tok_s.at[n], tok_r.at[slot, k], {"y": to})

    def tok_arrived(slot, k):
        tok_copy(part(slot, k), slot, k, 0, above).wait_recv()

    def w_copy(to, k, n):
        src = (wq, wk, wv)[n].at[:, pl.ds(pl.multiple_of(to * HEAD, HEAD), HEAD)]
        dst = wbuf.at[z, y, c, :, pl.ds(n * HEAD, HEAD)]
        return rcopy(src, dst, wy_s.at[k, n], wy_r.at[y, n], {"y": to})

    for k in range(1, NY):
        for n in range(3):
            w_copy(lax.rem(y + k, NY), k - 1, n).start()
    own = [
        tok_copy(tok.at[pl.ds(0, half), :], y, 0, 0, above),
        tok_copy(tok.at[pl.ds(half, half), :], y, 1, 1, below),
        tok_copy(tok.at[pl.ds(half, half), :], y, 1, 2, above),
        tok_copy(tok.at[pl.ds(0, half), :], y, 0, 3, below),
    ]
    for copy in own:
        copy.start()

    mine = pl.ds(pl.multiple_of(y * HEAD, HEAD), HEAD)
    for n, w in enumerate((wq, wk, wv)):
        wbuf[z, y, c, :, n * HEAD : (n + 1) * HEAD] = w[:, mine]
    xbuf[y] = tok[...]
    acc[...] = jnp.zeros_like(acc)
    top[...] = jnp.full_like(top, LOW)

    for k in range(1, NY):
        frm = lax.rem(y + k, NY)
        for n in range(3):
            dst = wbuf.at[z, frm, c, :, pl.ds(n * HEAD, HEAD)]
            rcopy(dst, dst, wy_s.at[k - 1, n], wy_r.at[frm, n], {"y": frm}).wait_recv()

    wring = ZRing(lambda o, cc, kind: wbuf.at[o, pl.ds(2 * kind, 2), cc], w_s, w_r, w_sib)
    for kind in (0, 1):
        wring.begin(kind)
    fwd_up = tok_copy(part(below, 0), below, 0, 4, above)
    fwd_down = tok_copy(part(above, 1), above, 1, 5, below)
    for d in range(1, NZ // 2 + 1):
        for kind in (0, 1):
            for way in (0, 1):
                if d <= wring.farthest(way, kind):
                    wring.pass_on(way, d, kind)
        if d == 2:
            tok_arrived(below, 0)
            fwd_up.start()
            tok_arrived(above, 1)
            fwd_down.start()
    for o in range(NZ):
        for kind in (0, 1):
            wring.arrived(o, 1 - c, kind)

    def project(i, carry):
        away = jnp.where(i == 2, 3, jnp.where(i == 3, 2, i))
        slot = lax.rem(y + away, NY)

        @pl.when(i == 1)
        def _():
            tok_arrived(above, 0)

        @pl.when(i == 2)
        def _():
            tok_arrived(below, 1)

        @pl.when(i == 3)
        def _():
            tok_arrived(across, 0)
            tok_arrived(across, 1)

        made = jnp.dot(
            xbuf[slot], wbuf[...].reshape(-1, 3 * HEAD), preferred_element_type=jnp.float32
        ).astype(jnp.bfloat16)
        at = pl.ds(pl.multiple_of(slot * ROWS, ROWS), ROWS)
        qrow[at, :] = made[:, :HEAD]
        kbuf[z, c, at, :] = made[:, HEAD : 2 * HEAD]
        vrow[at, :] = made[:, 2 * HEAD :]
        return carry

    lax.fori_loop(0, NY, project, 0)
    vbuf[z, c] = vrow[...].T

    ring = ZRing(lambda o, cc, kind: (kbuf, vbuf)[kind].at[o, cc], kv_s, kv_r, kv_sib)
    for kind in (0, 1):
        ring.begin(kind)

    q_t = qrow[...].T
    first = lax.broadcasted_iota(jnp.int32, q_t.shape, 0) < HEAD // 2
    zero = jnp.zeros_like(q_t)
    qbd[:, :TOKS] = jnp.where(first, q_t, zero)
    qbd[:, TOKS:] = jnp.where(first, zero, q_t)

    ones = jnp.ones((16, TOKS), jnp.bfloat16)

    def visit(o, cc, masked):
        keys = kbuf[o, cc]
        values = jnp.concatenate([vbuf[o, cc], ones], axis=0)
        for j in range(COLS // TILE):
            cols = slice(j * TILE, (j + 1) * TILE)
            s = jnp.dot(keys, qbd[:, cols], preferred_element_type=jnp.float32)
            if masked:
                u = lax.broadcasted_iota(jnp.int32, (TOKS, 1), 0)
                t = lax.broadcasted_iota(jnp.int32, (1, TILE), 1) + j * TILE
                t = jnp.where(t >= TOKS, t - TOKS, t)

                def place(r, core):
                    skipped = sum((r >= k * ROWS).astype(jnp.int32) for k in range(1, NY))
                    return r + ROWS * (skipped + core)

                s = jnp.where(place(u, cc) <= place(t, c), s, LOW)
            before = top[0:1, cols]
            now = jnp.maximum(before, jnp.max(s, axis=0, keepdims=True))
            shrink = jnp.exp2((before - now) * EXP_SCALE)
            p = jnp.exp2((s - now) * EXP_SCALE).astype(jnp.bfloat16)
            acc[:, cols] = acc[:, cols] * shrink + jnp.dot(values, p, preferred_element_type=jnp.float32)
            top[0:1, cols] = now

    def own_slice(k, carry):
        cc = jnp.where(k == 0, c, 1 - c)

        @pl.when(k == 1)
        def _():
            for kind in (0, 1):
                ring.arrived(z, 1 - c, kind)

        visit(z, cc, True)
        return carry

    lax.fori_loop(0, NC, own_slice, 0)

    def step(d, carry):
        for kind in (0, 1):
            for way in (0, 1):
                @pl.when(d <= ring.farthest(way, kind))
                def _():
                    ring.pass_on(way, d, kind)

            way = kind
            before = d - 1
            o = ring.origin(way, before)
            there = (before >= 1) & (before <= NZ // 2 - way)

            @pl.when(there)
            def _():
                for other in (0, 1):
                    ring.arrived(o, 1 - c, other)

            @pl.when(there & (o < z))
            def _():
                def both(cc, carry):
                    visit(o, cc, False)
                    return carry

                lax.fori_loop(0, NC, both, 0)

        return carry

    lax.fori_loop(1, NZ // 2 + 2, step, 0)

    def part_of(cols):
        return acc[:HEAD, cols] / acc[HEAD : HEAD + 1, cols]

    mixture = part_of(slice(0, TOKS)) - lam[y] * part_of(slice(TOKS, COLS))
    scale = lax.rsqrt(jnp.mean(mixture * mixture, axis=0, keepdims=True) + 1e-05)
    out[...] = (mixture * scale * gain[...]).T.astype(jnp.bfloat16)

    for copy in own + [fwd_up, fwd_down]:
        copy.wait_send()
    for k in range(1, NY):
        for n in range(3):
            w_copy(lax.rem(y + k, NY), k - 1, n).wait_send()
    wring.drain()
    ring.drain()


def attention(tokens, wq, wk, wv, lam, gain):
    vmem = pl.BlockSpec(memory_space=pltpu.VMEM)
    dma = pltpu.SemaphoreType.DMA
    width = tokens.shape[1]
    ring_sems = [dma((2, NZ // 2, 2)), dma((NZ, NC, 2)), dma((NZ, 2))]
    return pl.pallas_call(
        attention_kernel,
        out_shape=jax.ShapeDtypeStruct((TOKS, HEAD), jnp.bfloat16),
        in_specs=[vmem, vmem, vmem, vmem, pl.BlockSpec(memory_space=pltpu.SMEM), vmem],
        out_specs=vmem,
        scratch_shapes=[
            pltpu.VMEM((NY, ROWS, width), jnp.bfloat16),
            pltpu.VMEM((NZ, NY, NC, wq.shape[0], 3 * HEAD), jnp.bfloat16),
            pltpu.VMEM((NZ, NC, TOKS, HEAD), jnp.bfloat16),
            pltpu.VMEM((NZ, NC, HEAD, TOKS), jnp.bfloat16),
            pltpu.VMEM((TOKS, HEAD), jnp.bfloat16),
            pltpu.VMEM((TOKS, HEAD), jnp.bfloat16),
            pltpu.VMEM((HEAD, COLS), jnp.bfloat16),
            pltpu.VMEM((HEAD + 16, COLS), jnp.float32),
            pltpu.VMEM((8, COLS), jnp.float32),
            dma((6,)),
            dma((NY, 2)),
            dma((NY - 1, 3)),
            dma((NY, 3)),
            *ring_sems,
            *ring_sems,
        ],
        compiler_params=pltpu.CompilerParams(
            collective_id=0, has_side_effects=True, vmem_limit_bytes=56 * 1024 * 1024
        ),
        name="attention",
    )(tokens, wq, wk, wv, lam, gain.reshape(-1, 1))


def on_device(tokens, query_weight, key_weight, value_weight, out_weight, mix_lambda, head_gain):
    head_out = attention(tokens, query_weight, key_weight, value_weight, mix_lambda, head_gain)
    mine = lax.all_to_all(head_out.reshape(NY, ROWS, HEAD), "y", 0, 0)
    mine = jnp.transpose(mine, (1, 0, 2)).reshape(ROWS, NY * HEAD)
    out_t = lax.all_gather(out_weight.T, ("z", "y", "core"), axis=0, tiled=True)
    partial_out = lax.dot_general(mine, out_t, (((1,), (1,)), ((), ())), preferred_element_type=jnp.float32)
    own = lax.psum_scatter(partial_out.astype(jnp.bfloat16), "x", scatter_dimension=0, tiled=True)
    return lax.all_gather(own, "x", axis=0, tiled=True)


def solution(mesh):
    fine = Mesh(mesh.devices.reshape(NZ, NY, NC, NX), ("z", "y", "core", "x"))
    sp = ("z", "y", "core")
    placed = (P(sp, None), P(sp, "x"), P(sp, "x"), P(sp, "x"), P("x", sp), P("x"), P())
    return jax.shard_map(on_device, mesh=fine, in_specs=placed, out_specs=P(sp, None), check_vma=False)
```

time: 383 us -> 149 us (0.39)
  waiting for transfers between devices: 209 us -> 22.5 us
  Pallas kernels: 0 us -> 81.8 us
  matrix products: 75.1 us -> 3.26 us
  local copies, waits for them, and re-layouts: 39 us -> 2.23 us
  other arithmetic: 28.4 us -> 0 us
  blocking collectives: 13.2 us -> 22.7 us
    all_gather x2 -> x1, waiting for transfers between devices: 186 us -> 0.01 us  [on_device(): out_t = lax.all_gather(out_weight.T, ('z', 'y', 'core'), axis=0, tiled=True)]
    pallas_call x0 -> x1, Pallas kernels: none -> 81.8 us  [attention(): pl.pallas_call(attention_kernel, out_shape=jax.ShapeDtypeStruct((TOKS, HE...]
    dot_general x8 -> x1, matrix products: 75.1 us -> 3.26 us  [on_device(): lax.dot_general(mine, out_t, (((1,), (1,)), ((), ())), preferred_element_...]
    reduce_sum x3 -> x0, other arithmetic: 24.7 us -> none  [the longest x2 24.3 us: attend(): totals = jnp.sum(weights, axis=-1)]
    slice x7 -> x0, local copies, waits for them, and re-layouts: 20.9 us -> none  [the longest x1 19.5 us: sent_together(): slab = out[..., at:at + column.shape[along]]]
    unnamed x10 -> x1, local copies, waits for them, and re-layouts: 17.7 us -> 0.84 us
    all_to_all x0 -> x1, blocking collectives: none -> 9.48 us  [on_device(): mine = lax.all_to_all(head_out.reshape(NY, ROWS, HEAD), 'y', 0, 0)]
  transfers between devices with their start and end apart: 3 -> 2, of which waited for: 3 -> 1; matrix products, arithmetic and copies ran while one was open for 1% -> 1% of each run, Pallas kernels for 0% -> 56%
where the time goes in v1:
time: 149 us; the launch traced here: 146 us
  Pallas kernels  81.8 us (55%)
  blocking collectives  22.7 us (15%)
  waiting for transfers between devices  22.5 us (15%)
  between operations  13.4 us (9%)
  matrix products  3.26 us (2%)
  local copies, waits for them, and re-layouts  2.23 us (1%)
    pallas_call x1, Pallas kernels, attention(): pl.pallas_call(attention_kernel, out_shape=jax.ShapeDtypeStruct((TOKS, HE...  81.8 us
    reduce_scatter x1, waiting for transfers between devices, on_device(): lax.psum_scatter(partial_out.astype(jnp.bfloat16), 'x', scatter_dimension...  21.8 us
    all_gather x1, blocking collectives, on_device(): return lax.all_gather(own, 'x', axis=0, tiled=True)  13.2 us
    all_to_all x1, blocking collectives, on_device(): mine = lax.all_to_all(head_out.reshape(NY, ROWS, HEAD), 'y', 0, 0)  9.48 us
    dot_general x1, matrix products, on_device(): lax.dot_general(mine, out_t, (((1,), (1,)), ((), ())), preferred_element_...  3.26 us
  transfers between devices with their start and end apart: 2, of which 1 were waited for; matrix products, arithmetic and copies ran while one was open for 1% of the time, Pallas kernels for 56%

profile of v1, /device:TPU:224, one launch (start us, length us, event | category | flops | bytes accessed | tf_op | source)
XLA Modules:
  0.0 145.9 jit_solution(7796100266763011062)
XLA Ops:
  6.5 0.0 all-gather.2.cloned.1.call-start
  6.5 0.7 all-gather.2.cloned.1.call-update
  7.3 0.0 reduce-scatter.2.cloned.1.call-start
  7.3 1.4 copy.11.gain
  8.7 81.8 %attention.1 = bf16[640,128]{1,0:T(8,128)(2,1)} custom-call(bf16[160,2048]{1,0:T(8,128)(2,1)} %tok.1, bf16[32,512]{1,0:T(8,128)(2,1)} %wq.1, bf16[32,512]{1,0:T(8,128)(2,1)} %wk.1, bf16[32,512]{1,0:T(8,128)(2,1)} %wv.1, f32[4]{0:T(128)} %lam.1, f32[128,1]{1,0:T(8,128)} %copy.11.gain), custom_call_target="tpu_custom_call" | custom-call | tf_op jit(solution)/shard_map/attention/pallas_call | solution.py:282
  90.5 9.5 %all_to_all.5 = bf16[4,160,128]{2,1,0:T(8,128)(2,1)S(1)} all-to-all(bf16[4,160,128]{2,1,0:T(8,128)(2,1)} %bitcast.12), channel_id=1, replica_groups=mesh['z'=8,'y'=4,'core'=2,'x'=4] {'y'}, dimensions={0} | all-to-all | bytes 327680 | tf_op jit(solution)/shard_map/all_to_all | solution.py:313
  99.9 0.0 all-gather.2.cloned.1.call-done
  99.9 3.3 %convolution_convert_fusion = bf16[160,2048]{1,0:T(8,128)(2,1)} fusion(bf16[2048,512]{1,0:T(8,128)(2,1)} %all-gather.2.cloned.1.call-done, bf16[4,160,128]{2,1,0:T(8,128)(2,1)S(1)} %all_to_all.5), kind=kOutput, calls=%fused_computation | convolution fusion | flops 335872000 | bytes 2916352 | tf_op jit(solution)/shard_map/dot_general | solution.py:316
  103.2 0.0 reduce-scatter.2.cloned.1.call-update
  103.2 21.8 %reduce-scatter.2.cloned.1.call-done = bf16[40,2048]{1,0:T(8,128)(2,1)} async-done(((bf16[160,2048]{1,0:T(8,128)(2,1)}), bf16[40,2048]{1,0:T(8,128)(2,1)}) %reduce-scatter.2.cloned.1.call-update) | async-done | bytes 163856 | tf_op jit(solution)/shard_map/reduce_scatter | solution.py:317
  125.0 13.2 %all_gather.7 = bf16[160,2048]{1,0:T(8,128)(2,1)S(1)} all-gather(bf16[40,2048]{1,0:T(8,128)(2,1)} %reduce-scatter.2.cloned.1.call-done), channel_id=1, replica_groups=mesh['z'=8,'y'=4,'core'=2,'x'=4] {'x'}, dimensions={0}, use_global_device_ids=true | all-gather | bytes 819200 | tf_op jit(solution)/shard_map/all_gather | solution.py:318
  138.2 0.8 copy.19
Async XLA Ops:
  6.5 93.4 %all-gather.2.cloned.1.call-start = ((), (), s32[]{:S(2)}) async-start(), calls=%async_computation.2 | async-start | bytes 2129920 | tf_op jit(solution)/shard_map/all_gather | solution.py:315
  7.3 117.7 %reduce-scatter.2.cloned.1.call-start = ((), (), s32[]{:S(2)}) async-start(), calls=%async_computation.3 | async-start | bytes 819200 | tf_op jit(solution)/shard_map/reduce_scatter | solution.py:317
Sparse Core Ops, SparseCore 0:
  10.1 76.6 all-gather.1
  103.3 21.5 reduce-scatter.1

commit v2 on v1

--- a/solution.py
+++ b/solution.py
@@ -77,17 +77,21 @@
 
 
 def attention_kernel(
-    tok, wq, wk, wv, lam, gain, out,
-    xbuf, wbuf, kbuf, vbuf, qrow, vrow, qbd, acc, top,
+    tok, wq, wk, wv, wo, lam, gain, out,
+    xbuf, wbuf, kbuf, vbuf, qrow, vrow, qbd, acc, top, wt, hrow, hbuf,
     tok_s, tok_r, wy_s, wy_r, w_s, w_r, w_sib, kv_s, kv_r, kv_sib,
+    oz_s, oz_r, oy_s, oy_r, ox_s, of_s, ox_r, oc_s, oc_r, h_s, hf_s, h_r, hf_r,
 ):
-    z, y, c = lax.axis_index("z"), lax.axis_index("y"), lax.axis_index("core")
+    z, y, c, x = (lax.axis_index(name) for name in ("z", "y", "core", "x"))
+    right, left, facing = lax.rem(x + 1, NX), lax.rem(x + NX - 1, NX), lax.rem(x + 2, NX)
     above, below = lax.rem(y + 1, NY), lax.rem(y + NY - 1, NY)
     across = lax.rem(y + 2, NY)
 
     barrier = pltpu.get_barrier_semaphore()
     friends = [{"y": lax.rem(y + k, NY)} for k in range(1, NY)]
-    friends += [{"z": lax.rem(z + 1, NZ)}, {"z": lax.rem(z + NZ - 1, NZ)}, {"core": 1 - c}]
+    friends += [{"z": lax.rem(z + k, NZ)} for k in range(1, NZ)]
+    friends += [{"y": lax.rem(y + k, NY), "x": to} for k in range(NY) for to in (left, right)]
+    friends += [{"core": 1 - c}]
     for friend in friends:
         pl.semaphore_signal(barrier, inc=1, device_id=friend, device_id_type=MESH)
     pl.semaphore_wait(barrier, len(friends))
@@ -119,6 +123,61 @@
     ]
     for copy in own:
         copy.start()
+
+    def piece(xx, yy):
+        return wt.at[xx, :, yy, c]
+
+    def half_piece(xx, yy, k):
+        return wt.at[xx, pl.ds(k * (NZ // 2), NZ // 2), yy, c]
+
+    def turn(i):
+        return lax.rem(y + jnp.where(i == 2, 3, jnp.where(i == 3, 2, i)), NY)
+
+    def o_z(k):
+        block = wt.at[x, z, y, c]
+        return rcopy(block, block, oz_s.at[k - 1], oz_r.at[z], {"z": lax.rem(z + k, NZ)})
+
+    def o_z_arrived(k):
+        frm = lax.rem(z + k, NZ)
+        block = wt.at[x, frm, y, c]
+        rcopy(block, block, oz_s.at[k - 1], oz_r.at[frm], {"z": frm}).wait_recv()
+
+    def o_y(k):
+        return rcopy(piece(x, y), piece(x, y), oy_s.at[k - 1], oy_r.at[y], {"y": lax.rem(y + k, NY)})
+
+    def o_y_arrived(yy):
+        rcopy(piece(x, yy), piece(x, yy), oy_s.at[0], oy_r.at[yy], {"y": above}).wait_recv()
+
+    def o_x(yy):
+        return [
+            rcopy(half_piece(x, yy, k), half_piece(x, yy, k), ox_s.at[yy, n], ox_r.at[x, yy, k], {"x": to})
+            for n, (k, to) in enumerate([(0, right), (1, left), (1, right), (0, left)])
+        ]
+
+    def o_x_arrived(xx, yy, k):
+        ref = half_piece(xx, yy, k)
+        rcopy(ref, ref, ox_s.at[yy, 0], ox_r.at[xx, yy, k], {"x": right}).wait_recv()
+
+    def o_relay(yy, k):
+        frm, to = ((left, right), (right, left))[k]
+        ref = half_piece(frm, yy, k)
+        return rcopy(ref, ref, of_s.at[yy, k], ox_r.at[frm, yy, k], {"x": to})
+
+    def o_share(xx, yy):
+        return rcopy(piece(xx, yy), piece(xx, yy), oc_s.at[xx, yy], oc_r.at[xx, yy], {"core": 1 - c})
+
+    def o_shared(xx, yy):
+        ref = wt.at[xx, :, yy, 1 - c]
+        rcopy(ref, ref, oc_s.at[xx, yy], oc_r.at[xx, yy], {"core": 1 - c}).wait_recv()
+
+    def o_spread(yy):
+        for copy in o_x(yy):
+            copy.start()
+        o_share(x, yy).start()
+
+    wt[x, z, y, c] = wo[...].T
+    for k in range(1, NZ):
+        o_z(k).start()
 
     mine = pl.ds(pl.multiple_of(y * HEAD, HEAD), HEAD)
     for n, w in enumerate((wq, wk, wv)):
@@ -152,9 +211,14 @@
         for kind in (0, 1):
             wring.arrived(o, 1 - c, kind)
 
+    for k in range(1, NZ):
+        o_z_arrived(k)
+    for k in range(1, NY):
+        o_y(k).start()
+    o_spread(y)
+
     def project(i, carry):
-        away = jnp.where(i == 2, 3, jnp.where(i == 3, 2, i))
-        slot = lax.rem(y + away, NY)
+        slot = turn(i)
 
         @pl.when(i == 1)
         def _():
@@ -254,6 +318,21 @@
 
                 lax.fori_loop(0, NC, both, 0)
 
+        @pl.when(d < NY)
+        def _():
+            o_y_arrived(turn(d))
+            o_spread(turn(d))
+
+        @pl.when(d >= 2)
+        def _():
+            yy = turn(d - 2)
+            for k, frm in enumerate((left, right)):
+                o_x_arrived(frm, yy, k)
+                o_relay(yy, k).start()
+            for k, frm in enumerate((left, right)):
+                o_x_arrived(frm, yy, 1 - k)
+                o_share(frm, yy).start()
+
         return carry
 
     lax.fori_loop(1, NZ // 2 + 2, step, 0)
@@ -263,7 +342,84 @@
 
     mixture = part_of(slice(0, TOKS)) - lam[y] * part_of(slice(TOKS, COLS))
     scale = lax.rsqrt(jnp.mean(mixture * mixture, axis=0, keepdims=True) + 1e-05)
-    out[...] = (mixture * scale * gain[...]).T.astype(jnp.bfloat16)
+    hrow[...] = ((mixture * scale).T * gain[...]).astype(jnp.bfloat16).reshape(NY, ROWS, HEAD)
+
+    def rows(k):
+        return pl.ds(k * half, half)
+
+    def h_copy(yy, k, n, device):
+        dst = hbuf.at[x, rows(k), pl.ds(pl.multiple_of(y * HEAD, HEAD), HEAD)]
+        return rcopy(hrow.at[yy, rows(k), :], dst, h_s.at[yy, n], h_r.at[x, y, k], device)
+
+    def h_arrived(xx, yy, k):
+        dst = hbuf.at[xx, rows(k), pl.ds(pl.multiple_of(yy * HEAD, HEAD), HEAD)]
+        rcopy(hrow.at[yy, rows(k), :], dst, h_s.at[yy, 0], h_r.at[xx, yy, k], {"x": right}).wait_recv()
+
+    def h_relay(k):
+        frm, to = ((left, right), (right, left))[k]
+        ref = hbuf.at[frm, rows(k), :]
+        return rcopy(ref, ref, hf_s.at[k], hf_r.at[k], {"x": to})
+
+    sent = []
+    for n, (k, to) in enumerate([(0, right), (1, left), (1, right), (0, left)]):
+        for i in range(NY):
+            yy = lax.rem(y + i, NY)
+            sent.append(h_copy(yy, k, n, {"y": yy, "x": to}))
+            sent[-1].start()
+        if n == 1:
+            for i in range(1, NY):
+                yy = lax.rem(y + i, NY)
+                for kk in (0, 1):
+                    sent.append(h_copy(yy, kk, 4 + kk, {"y": yy}))
+                    sent[-1].start()
+    hbuf[x, :, mine] = hrow[y]
+    relays = [h_relay(0), h_relay(1)]
+    for k, frm in enumerate((left, right)):
+        for i in range(NY):
+            h_arrived(frm, lax.rem(y + i, NY), k)
+        relays[k].start()
+
+    for i in range(NY):
+        yy = turn(i)
+        for k in (0, 1):
+            o_x_arrived(facing, yy, k)
+        o_share(facing, yy).start()
+    for xx in range(NX):
+        for yy in range(NY):
+            o_shared(xx, yy)
+    for k in (0, 1):
+        for i in range(1, NY):
+            h_arrived(x, lax.rem(y + i, NY), k)
+    for k, frm in enumerate((left, right)):
+        for i in range(NY):
+            h_arrived(frm, lax.rem(y + i, NY), 1 - k)
+    for k in (0, 1):
+        ref = hbuf.at[facing, rows(k), :]
+        rcopy(ref, ref, hf_s.at[k], hf_r.at[k], {"x": right}).wait_recv()
+
+    width = wo.shape[0]
+    for j in range(out.shape[1] // width):
+        total = jnp.zeros((width, ROWS), jnp.float32)
+        for xx in range(NX):
+            block = wt[xx, 2 * j : 2 * j + 2].reshape(width, width)
+            total += lax.dot_general(
+                block, hbuf[xx], (((1,), (1,)), ((), ())), preferred_element_type=jnp.float32
+            )
+        out[:, j * width : (j + 1) * width] = total.T.astype(jnp.bfloat16)
+
+    for copy in sent + relays:
+        copy.wait_send()
+    for k in range(1, NZ):
+        o_z(k).wait_send()
+    for k in range(1, NY):
+        o_y(k).wait_send()
+    for yy in range(NY):
+        for copy in o_x(yy):
+            copy.wait_send()
+        for k in (0, 1):
+            o_relay(yy, k).wait_send()
+        for xx in range(NX):
+            o_share(xx, yy).wait_send()
 
     for copy in own + [fwd_up, fwd_down]:
         copy.wait_send()
@@ -274,15 +430,15 @@
     ring.drain()
 
 
-def attention(tokens, wq, wk, wv, lam, gain):
+def attention(tokens, wq, wk, wv, wo, lam, gain):
     vmem = pl.BlockSpec(memory_space=pltpu.VMEM)
     dma = pltpu.SemaphoreType.DMA
     width = tokens.shape[1]
     ring_sems = [dma((2, NZ // 2, 2)), dma((NZ, NC, 2)), dma((NZ, 2))]
     return pl.pallas_call(
         attention_kernel,
-        out_shape=jax.ShapeDtypeStruct((TOKS, HEAD), jnp.bfloat16),
-        in_specs=[vmem, vmem, vmem, vmem, pl.BlockSpec(memory_space=pltpu.SMEM), vmem],
+        out_shape=jax.ShapeDtypeStruct(tokens.shape, jnp.bfloat16),
+        in_specs=[vmem, vmem, vmem, vmem, vmem, pl.BlockSpec(memory_space=pltpu.SMEM), vmem],
         out_specs=vmem,
         scratch_shapes=[
             pltpu.VMEM((NY, ROWS, width), jnp.bfloat16),
@@ -294,28 +450,38 @@
             pltpu.VMEM((HEAD, COLS), jnp.bfloat16),
             pltpu.VMEM((HEAD + 16, COLS), jnp.float32),
             pltpu.VMEM((8, COLS), jnp.float32),
+            pltpu.VMEM((NX, NZ, NY, NC, wo.shape[1], wo.shape[0]), jnp.bfloat16),
+            pltpu.VMEM((NY, ROWS, HEAD), jnp.bfloat16),
+            pltpu.VMEM((NX, ROWS, NY * HEAD), jnp.bfloat16),
             dma((6,)),
             dma((NY, 2)),
             dma((NY - 1, 3)),
             dma((NY, 3)),
             *ring_sems,
             *ring_sems,
+            dma((NZ - 1,)),
+            dma((NZ,)),
+            dma((NY - 1,)),
+            dma((NY,)),
+            dma((NY, 4)),
+            dma((NY, 2)),
+            dma((NX, NY, 2)),
+            dma((NX, NY)),
+            dma((NX, NY)),
+            dma((NY, 6)),
+            dma((2,)),
+            dma((NX, NY, 2)),
+            dma((2,)),
         ],
         compiler_params=pltpu.CompilerParams(
             collective_id=0, has_side_effects=True, vmem_limit_bytes=56 * 1024 * 1024
         ),
         name="attention",
-    )(tokens, wq, wk, wv, lam, gain.reshape(-1, 1))
+    )(tokens, wq, wk, wv, wo, lam, gain.reshape(1, -1))
 
 
 def on_device(tokens, query_weight, key_weight, value_weight, out_weight, mix_lambda, head_gain):
-    head_out = attention(tokens, query_weight, key_weight, value_weight, mix_lambda, head_gain)
-    mine = lax.all_to_all(head_out.reshape(NY, ROWS, HEAD), "y", 0, 0)
-    mine = jnp.transpose(mine, (1, 0, 2)).reshape(ROWS, NY * HEAD)
-    out_t = lax.all_gather(out_weight.T, ("z", "y", "core"), axis=0, tiled=True)
-    partial_out = lax.dot_general(mine, out_t, (((1,), (1,)), ((), ())), preferred_element_type=jnp.float32)
-    own = lax.psum_scatter(partial_out.astype(jnp.bfloat16), "x", scatter_dimension=0, tiled=True)
-    return lax.all_gather(own, "x", axis=0, tiled=True)
+    return attention(tokens, query_weight, key_weight, value_weight, out_weight, mix_lambda, head_gain)
 
 
 def solution(mesh):

time: 149 us -> 105 us (0.70); the launches traced: 146 us -> 104 us
  blocking collectives: 22.7 us -> 0 us
  waiting for transfers between devices: 22.5 us -> 0 us
  Pallas kernels: 81.8 us -> 101 us
  between operations: 13.4 us -> 0.01 us
  matrix products: 3.26 us -> 0 us
    reduce_scatter x1 -> x0, waiting for transfers between devices: 21.8 us -> none  [on_device(): lax.psum_scatter(partial_out.astype(jnp.bfloat16), 'x', scatter_dimension...]
    pallas_call x1, Pallas kernels: 81.8 us -> 101 us  [attention(): pl.pallas_call(attention_kernel, out_shape=jax.ShapeDtypeStruct(tokens.sh...]
    all_gather x1 -> x0, blocking collectives: 13.2 us -> none  [on_device(): return lax.all_gather(own, 'x', axis=0, tiled=True)]
    all_to_all x1 -> x0, blocking collectives: 9.48 us -> none  [on_device(): mine = lax.all_to_all(head_out.reshape(NY, ROWS, HEAD), 'y', 0, 0)]
    dot_general x1 -> x0, matrix products: 3.26 us -> none  [on_device(): lax.dot_general(mine, out_t, (((1,), (1,)), ((), ())), preferred_element_...]
    unnamed x1 -> x2, local copies, waits for them, and re-layouts: 0.84 us -> 3.5 us
  transfers between devices with their start and end apart: 2 -> 0, of which waited for: 1 -> 0; matrix products, arithmetic and copies ran while one was open for 1% -> 0% of each run, Pallas kernels for 56% -> 0%
where the time goes in v2:
time: 105 us; the launch traced here: 104 us
  Pallas kernels  101 us (96%)
  local copies, waits for them, and re-layouts  3.5 us (3%)
    pallas_call x1, Pallas kernels, attention(): pl.pallas_call(attention_kernel, out_shape=jax.ShapeDtypeStruct(tokens.sh...  101 us
    unnamed x2, local copies, waits for them, and re-layouts  3.5 us

profile of v2, /device:TPU:224, one launch (start us, length us, event | category | flops | bytes accessed | tf_op | source)
XLA Modules:
  0.0 104.3 jit_solution(14926348966208463141)
XLA Ops:
  0.0 1.5 %copy.8.wo = bf16[512,32]{1,0:T(8,128)(2,1)} copy(bf16[512,32]{0,1:T(8,128)(2,1)} %param.11) | data formatting | bytes 65536 | tf_op args[4]
  1.5 100.8 %attention.1 = bf16[160,2048]{1,0:T(8,128)(2,1)} custom-call(bf16[160,2048]{1,0:T(8,128)(2,1)} %tok.1, bf16[32,512]{1,0:T(8,128)(2,1)} %wq.1, bf16[32,512]{1,0:T(8,128)(2,1)} %wk.1, bf16[32,512]{1,0:T(8,128)(2,1)} %wv.1, bf16[512,32]{1,0:T(8,128)(2,1)} %copy.8.wo, f32[4]{0:T(128)} %lam.1, f32[1,128]{1,0:T(1,128)} %bitcast.1), custom_call_target="tpu_custom_call" | custom-call | tf_op jit(solution)/shard_map/attention/pallas_call | solution.py:438
  102.3 2.0 %copy.10 = bf16[160,2048]{1,0:T(8,128)(2,1)} copy(bf16[160,2048]{1,0:T(8,128)(2,1)} %attention.1) | data formatting | bytes 1310720

commit v3 on v2

--- a/solution.py
+++ b/solution.py
@@ -16,6 +16,7 @@
 HEAD = 128
 COLS = 2 * TOKS
 TILE = 256
+KINDS = 4
 LOW = -1e30
 EXP_SCALE = 64 ** (-0.5) * math.log2(math.e)
 
@@ -35,7 +36,7 @@
         return lax.rem(self.z + (NZ - d if way == 0 else d), NZ)
 
     def farthest(self, way, kind):
-        return NZ // 2 - (way != kind)
+        return NZ // 2 - (way != kind % 2)
 
     def onward(self, way, d, kind, o):
         ref = self.block(o, self.c, kind)
@@ -66,7 +67,7 @@
         self.share(o, kind).start()
 
     def drain(self):
-        for kind in (0, 1):
+        for kind in range(KINDS):
             for way in (0, 1):
                 for d in range(1, self.farthest(way, kind) + 1):
                     self.onward(way, d, kind, self.z).wait_send()
@@ -78,7 +79,7 @@
 
 def attention_kernel(
     tok, wq, wk, wv, wo, lam, gain, out,
-    xbuf, wbuf, kbuf, vbuf, qrow, vrow, qbd, acc, top, wt, hrow, hbuf,
+    xbuf, wkv, wqs, kv, qrow, qbd, acc, top, wt, hrow, hbuf, osum,
     tok_s, tok_r, wy_s, wy_r, w_s, w_r, w_sib, kv_s, kv_r, kv_sib,
     oz_s, oz_r, oy_s, oy_r, ox_s, of_s, ox_r, oc_s, oc_r, h_s, hf_s, h_r, hf_r,
 ):
@@ -107,14 +108,22 @@
     def tok_arrived(slot, k):
         tok_copy(part(slot, k), slot, k, 0, above).wait_recv()
 
-    def w_copy(to, k, n):
+    def w_slot(frm, n):
+        return (wqs.at[z, frm, c], wkv.at[z, frm, c, :, pl.ds(0, HEAD)], wkv.at[z, frm, c, :, pl.ds(HEAD, HEAD)])[n]
+
+    def w_copy(k, n):
+        to = lax.rem(y + k, NY)
         src = (wq, wk, wv)[n].at[:, pl.ds(pl.multiple_of(to * HEAD, HEAD), HEAD)]
-        dst = wbuf.at[z, y, c, :, pl.ds(n * HEAD, HEAD)]
-        return rcopy(src, dst, wy_s.at[k, n], wy_r.at[y, n], {"y": to})
-
-    for k in range(1, NY):
-        for n in range(3):
-            w_copy(lax.rem(y + k, NY), k - 1, n).start()
+        return rcopy(src, w_slot(y, n), wy_s.at[k - 1, n], wy_r.at[y, n], {"y": to})
+
+    def w_arrived(n):
+        for k in range(1, NY):
+            frm = lax.rem(y + k, NY)
+            rcopy(w_slot(frm, n), w_slot(frm, n), wy_s.at[k - 1, n], wy_r.at[frm, n], {"y": frm}).wait_recv()
+
+    for n in (1, 2, 0):
+        for k in range(1, NY):
+            w_copy(k, n).start()
     own = [
         tok_copy(tok.at[pl.ds(0, half), :], y, 0, 0, above),
         tok_copy(tok.at[pl.ds(half, half), :], y, 1, 1, below),
@@ -175,33 +184,40 @@
             copy.start()
         o_share(x, yy).start()
 
-    wt[x, z, y, c] = wo[...].T
-    for k in range(1, NZ):
-        o_z(k).start()
+    wt[x, z, y, c] = wo[...]
 
     mine = pl.ds(pl.multiple_of(y * HEAD, HEAD), HEAD)
-    for n, w in enumerate((wq, wk, wv)):
-        wbuf[z, y, c, :, n * HEAD : (n + 1) * HEAD] = w[:, mine]
+    wqs[z, y, c] = wq[:, mine]
+    wkv[z, y, c, :, :HEAD] = wk[:, mine]
+    wkv[z, y, c, :, HEAD:] = wv[:, mine]
     xbuf[y] = tok[...]
     acc[...] = jnp.zeros_like(acc)
     top[...] = jnp.full_like(top, LOW)
 
-    for k in range(1, NY):
-        frm = lax.rem(y + k, NY)
-        for n in range(3):
-            dst = wbuf.at[z, frm, c, :, pl.ds(n * HEAD, HEAD)]
-            rcopy(dst, dst, wy_s.at[k - 1, n], wy_r.at[frm, n], {"y": frm}).wait_recv()
-
-    wring = ZRing(lambda o, cc, kind: wbuf.at[o, pl.ds(2 * kind, 2), cc], w_s, w_r, w_sib)
+    w_ring = ZRing(lambda o, cc, kind: (wkv, wqs)[kind // 2].at[o, pl.ds(2 * (kind % 2), 2), cc], w_s, w_r, w_sib)
+    ring = ZRing(lambda o, cc, kind: kv.at[o, cc, pl.ds(kind * ROWS, ROWS), :], kv_s, kv_r, kv_sib)
+
+    def pass_all(what, d, kinds):
+        for kind in kinds:
+            for way in (0, 1):
+                if d <= what.farthest(way, kind):
+                    what.pass_on(way, d, kind)
+
+    w_arrived(1)
+    w_arrived(2)
     for kind in (0, 1):
-        wring.begin(kind)
+        w_ring.begin(kind)
+    w_arrived(0)
+    for kind in (2, 3):
+        w_ring.begin(kind)
     fwd_up = tok_copy(part(below, 0), below, 0, 4, above)
     fwd_down = tok_copy(part(above, 1), above, 1, 5, below)
     for d in range(1, NZ // 2 + 1):
-        for kind in (0, 1):
-            for way in (0, 1):
-                if d <= wring.farthest(way, kind):
-                    wring.pass_on(way, d, kind)
+        pass_all(w_ring, d, (0, 1))
+        if d > 1:
+            pass_all(w_ring, d - 1, (2, 3))
+        for k in {d, NZ - d}:
+            o_z(k).start()
         if d == 2:
             tok_arrived(below, 0)
             fwd_up.start()
@@ -209,46 +225,51 @@
             fwd_down.start()
     for o in range(NZ):
         for kind in (0, 1):
-            wring.arrived(o, 1 - c, kind)
-
+            w_ring.arrived(o, 1 - c, kind)
+
+    def project(i):
+        at = pl.ds(pl.multiple_of(i * ROWS, ROWS), ROWS)
+        kv[z, c, at, :] = jnp.dot(
+            xbuf[turn(i)], wkv[...].reshape(-1, 2 * HEAD), preferred_element_type=jnp.float32
+        ).astype(jnp.bfloat16)
+        ring.begin(i)
+
+    def project_near(i, carry):
+        @pl.when(i == 1)
+        def _():
+            tok_arrived(above, 0)
+
+        @pl.when(i == 2)
+        def _():
+            tok_arrived(below, 1)
+
+        project(i)
+        return carry
+
+    lax.fori_loop(0, NY - 1, project_near, 0)
+
+    pass_all(w_ring, NZ // 2, (2, 3))
     for k in range(1, NZ):
         o_z_arrived(k)
     for k in range(1, NY):
         o_y(k).start()
     o_spread(y)
-
-    def project(i, carry):
-        slot = turn(i)
-
-        @pl.when(i == 1)
-        def _():
-            tok_arrived(above, 0)
-
-        @pl.when(i == 2)
-        def _():
-            tok_arrived(below, 1)
-
-        @pl.when(i == 3)
-        def _():
-            tok_arrived(across, 0)
-            tok_arrived(across, 1)
-
-        made = jnp.dot(
-            xbuf[slot], wbuf[...].reshape(-1, 3 * HEAD), preferred_element_type=jnp.float32
+    pass_all(ring, 1, range(NY - 1))
+    for o in range(NZ):
+        for kind in (2, 3):
+            w_ring.arrived(o, 1 - c, kind)
+    for k in (0, 1):
+        tok_arrived(across, k)
+    project(NY - 1)
+
+    def queries(i, carry):
+        at = pl.ds(pl.multiple_of(i * ROWS, ROWS), ROWS)
+        qrow[at, :] = jnp.dot(
+            xbuf[turn(i)], wqs[...].reshape(-1, HEAD), preferred_element_type=jnp.float32
         ).astype(jnp.bfloat16)
-        at = pl.ds(pl.multiple_of(slot * ROWS, ROWS), ROWS)
-        qrow[at, :] = made[:, :HEAD]
-        kbuf[z, c, at, :] = made[:, HEAD : 2 * HEAD]
-        vrow[at, :] = made[:, 2 * HEAD :]
         return carry
 
-    lax.fori_loop(0, NY, project, 0)
-    vbuf[z, c] = vrow[...].T
-
-    ring = ZRing(lambda o, cc, kind: (kbuf, vbuf)[kind].at[o, cc], kv_s, kv_r, kv_sib)
-    for kind in (0, 1):
-        ring.begin(kind)
-
+    lax.fori_loop(0, NY, queries, 0)
     q_t = qrow[...].T
     first = lax.broadcasted_iota(jnp.int32, q_t.shape, 0) < HEAD // 2
     zero = jnp.zeros_like(q_t)
@@ -257,21 +278,27 @@
 
     ones = jnp.ones((16, TOKS), jnp.bfloat16)
 
+    def place(r, core):
+        i = sum((r >= k * ROWS).astype(jnp.int32) for k in range(1, NY))
+        return r + ROWS * (2 * turn(i) - i + core)
+
     def visit(o, cc, masked):
-        keys = kbuf[o, cc]
-        values = jnp.concatenate([vbuf[o, cc], ones], axis=0)
+        keys = kv[o, cc, :, :HEAD]
+        values = jnp.concatenate([kv[o, cc, :, HEAD:].T, ones], axis=0)
+
+        def scores(j):
+            return jnp.dot(keys, qbd[:, j * TILE : (j + 1) * TILE], preferred_element_type=jnp.float32)
+
+        ahead = scores(0)
         for j in range(COLS // TILE):
             cols = slice(j * TILE, (j + 1) * TILE)
-            s = jnp.dot(keys, qbd[:, cols], preferred_element_type=jnp.float32)
+            s = ahead
+            if j + 1 < COLS // TILE:
+                ahead = scores(j + 1)
             if masked:
                 u = lax.broadcasted_iota(jnp.int32, (TOKS, 1), 0)
                 t = lax.broadcasted_iota(jnp.int32, (1, TILE), 1) + j * TILE
                 t = jnp.where(t >= TOKS, t - TOKS, t)
-
-                def place(r, core):
-                    skipped = sum((r >= k * ROWS).astype(jnp.int32) for k in range(1, NY))
-                    return r + ROWS * (skipped + core)
-
                 s = jnp.where(place(u, cc) <= place(t, c), s, LOW)
             before = top[0:1, cols]
             now = jnp.maximum(before, jnp.max(s, axis=0, keepdims=True))
@@ -285,7 +312,7 @@
 
         @pl.when(k == 1)
         def _():
-            for kind in (0, 1):
+            for kind in range(KINDS):
                 ring.arrived(z, 1 - c, kind)
 
         visit(z, cc, True)
@@ -294,20 +321,22 @@
     lax.fori_loop(0, NC, own_slice, 0)
 
     def step(d, carry):
-        for kind in (0, 1):
-            for way in (0, 1):
-                @pl.when(d <= ring.farthest(way, kind))
-                def _():
-                    ring.pass_on(way, d, kind)
-
-            way = kind
+        for way in (0, 1):
+            for kind in (2 * way, 2 * way + 1):
+                for course in (0, 1):
+                    due = d <= ring.farthest(course, kind)
+
+                    @pl.when(due if kind == KINDS - 1 else due & (d > 1))
+                    def _():
+                        ring.pass_on(course, d, kind)
+
             before = d - 1
             o = ring.origin(way, before)
             there = (before >= 1) & (before <= NZ // 2 - way)
 
             @pl.when(there)
             def _():
-                for other in (0, 1):
+                for other in range(KINDS):
                     ring.arrived(o, 1 - c, other)
 
             @pl.when(there & (o < z))
@@ -347,13 +376,13 @@
     def rows(k):
         return pl.ds(k * half, half)
 
-    def h_copy(yy, k, n, device):
+    def h_copy(i, k, n, device):
         dst = hbuf.at[x, rows(k), pl.ds(pl.multiple_of(y * HEAD, HEAD), HEAD)]
-        return rcopy(hrow.at[yy, rows(k), :], dst, h_s.at[yy, n], h_r.at[x, y, k], device)
+        return rcopy(hrow.at[i, rows(k), :], dst, h_s.at[i, n], h_r.at[x, y, k], {"y": turn(i), **device})
 
     def h_arrived(xx, yy, k):
         dst = hbuf.at[xx, rows(k), pl.ds(pl.multiple_of(yy * HEAD, HEAD), HEAD)]
-        rcopy(hrow.at[yy, rows(k), :], dst, h_s.at[yy, 0], h_r.at[xx, yy, k], {"x": right}).wait_recv()
+        rcopy(hrow.at[0, rows(k), :], dst, h_s.at[0, 0], h_r.at[xx, yy, k], {"x": right}).wait_recv()
 
     def h_relay(k):
         frm, to = ((left, right), (right, left))[k]
@@ -363,16 +392,14 @@
     sent = []
     for n, (k, to) in enumerate([(0, right), (1, left), (1, right), (0, left)]):
         for i in range(NY):
-            yy = lax.rem(y + i, NY)
-            sent.append(h_copy(yy, k, n, {"y": yy, "x": to}))
+            sent.append(h_copy(i, k, n, {"x": to}))
             sent[-1].start()
         if n == 1:
             for i in range(1, NY):
-                yy = lax.rem(y + i, NY)
                 for kk in (0, 1):
-                    sent.append(h_copy(yy, kk, 4 + kk, {"y": yy}))
+                    sent.append(h_copy(i, kk, 4 + kk, {}))
                     sent[-1].start()
-    hbuf[x, :, mine] = hrow[y]
+    hbuf[x, :, mine] = hrow[0]
     relays = [h_relay(0), h_relay(1)]
     for k, frm in enumerate((left, right)):
         for i in range(NY):
@@ -384,7 +411,7 @@
         for k in (0, 1):
             o_x_arrived(facing, yy, k)
         o_share(facing, yy).start()
-    for xx in range(NX):
+    for xx in (x, left, right):
         for yy in range(NY):
             o_shared(xx, yy)
     for k in (0, 1):
@@ -393,19 +420,22 @@
     for k, frm in enumerate((left, right)):
         for i in range(NY):
             h_arrived(frm, lax.rem(y + i, NY), 1 - k)
+
+    width = wo.shape[1]
+
+    def product(j, xx):
+        block = wt[xx, 2 * j : 2 * j + 2].reshape(width, width)
+        return lax.dot_general(block, hbuf[xx], (((1,), (1,)), ((), ())), preferred_element_type=jnp.float32)
+
+    for j in range(out.shape[1] // width):
+        osum[j] = product(j, x) + product(j, left) + product(j, right)
+    for yy in range(NY):
+        o_shared(facing, yy)
     for k in (0, 1):
         ref = hbuf.at[facing, rows(k), :]
         rcopy(ref, ref, hf_s.at[k], hf_r.at[k], {"x": right}).wait_recv()
-
-    width = wo.shape[0]
     for j in range(out.shape[1] // width):
-        total = jnp.zeros((width, ROWS), jnp.float32)
-        for xx in range(NX):
-            block = wt[xx, 2 * j : 2 * j + 2].reshape(width, width)
-            total += lax.dot_general(
-                block, hbuf[xx], (((1,), (1,)), ((), ())), preferred_element_type=jnp.float32
-            )
-        out[:, j * width : (j + 1) * width] = total.T.astype(jnp.bfloat16)
+        out[:, j * width : (j + 1) * width] = (osum[j] + product(j, facing)).T.astype(jnp.bfloat16)
 
     for copy in sent + relays:
         copy.wait_send()
@@ -425,8 +455,8 @@
         copy.wait_send()
     for k in range(1, NY):
         for n in range(3):
-            w_copy(lax.rem(y + k, NY), k - 1, n).wait_send()
-    wring.drain()
+            w_copy(k, n).wait_send()
+    w_ring.drain()
     ring.drain()
 
 
@@ -434,7 +464,7 @@
     vmem = pl.BlockSpec(memory_space=pltpu.VMEM)
     dma = pltpu.SemaphoreType.DMA
     width = tokens.shape[1]
-    ring_sems = [dma((2, NZ // 2, 2)), dma((NZ, NC, 2)), dma((NZ, 2))]
+    ring_sems = [dma((2, NZ // 2, KINDS)), dma((NZ, NC, KINDS)), dma((NZ, KINDS))]
     return pl.pallas_call(
         attention_kernel,
         out_shape=jax.ShapeDtypeStruct(tokens.shape, jnp.bfloat16),
@@ -442,17 +472,17 @@
         out_specs=vmem,
         scratch_shapes=[
             pltpu.VMEM((NY, ROWS, width), jnp.bfloat16),
-            pltpu.VMEM((NZ, NY, NC, wq.shape[0], 3 * HEAD), jnp.bfloat16),
-            pltpu.VMEM((NZ, NC, TOKS, HEAD), jnp.bfloat16),
-            pltpu.VMEM((NZ, NC, HEAD, TOKS), jnp.bfloat16),
-            pltpu.VMEM((TOKS, HEAD), jnp.bfloat16),
+            pltpu.VMEM((NZ, NY, NC, wq.shape[0], 2 * HEAD), jnp.bfloat16),
+            pltpu.VMEM((NZ, NY, NC, wq.shape[0], HEAD), jnp.bfloat16),
+            pltpu.VMEM((NZ, NC, TOKS, 2 * HEAD), jnp.bfloat16),
             pltpu.VMEM((TOKS, HEAD), jnp.bfloat16),
             pltpu.VMEM((HEAD, COLS), jnp.bfloat16),
             pltpu.VMEM((HEAD + 16, COLS), jnp.float32),
             pltpu.VMEM((8, COLS), jnp.float32),
-            pltpu.VMEM((NX, NZ, NY, NC, wo.shape[1], wo.shape[0]), jnp.bfloat16),
+            pltpu.VMEM((NX, NZ, NY, NC, wo.shape[0], wo.shape[1]), jnp.bfloat16),
             pltpu.VMEM((NY, ROWS, HEAD), jnp.bfloat16),
             pltpu.VMEM((NX, ROWS, NY * HEAD), jnp.bfloat16),
+            pltpu.VMEM((width // wo.shape[1], wo.shape[1], ROWS), jnp.float32),
             dma((6,)),
             dma((NY, 2)),
             dma((NY - 1, 3)),
@@ -481,7 +511,7 @@
 
 
 def on_device(tokens, query_weight, key_weight, value_weight, out_weight, mix_lambda, head_gain):
-    return attention(tokens, query_weight, key_weight, value_weight, out_weight, mix_lambda, head_gain)
+    return attention(tokens, query_weight, key_weight, value_weight, out_weight.T, mix_lambda, head_gain)
 
 
 def solution(mesh):

time: 105 us -> 92.6 us (0.88)
  the two profiles are of different devices: /device:TPU:224 before, /device:TPU:4 now
where the time goes in v3:
time: 92.6 us; the launch traced here: 92.5 us
  Pallas kernels  90.5 us (98%)
  local copies, waits for them, and re-layouts  1.98 us (2%)
    pallas_call x1, Pallas kernels, attention(): pl.pallas_call(attention_kernel, out_shape=jax.ShapeDtypeStruct(tokens.sh...  90.5 us
    unnamed x1, local copies, waits for them, and re-layouts  1.98 us

profile of v3, /device:TPU:4, one launch (start us, length us, event | category | flops | bytes accessed | tf_op | source)
XLA Modules:
  0.0 92.5 jit_solution(8083172530993922677)
XLA Ops:
  0.0 90.5 %attention.1 = bf16[160,2048]{1,0:T(8,128)(2,1)} custom-call(bf16[160,2048]{1,0:T(8,128)(2,1)} %tok.1, bf16[32,512]{1,0:T(8,128)(2,1)} %wq.1, bf16[32,512]{1,0:T(8,128)(2,1)} %wk.1, bf16[32,512]{1,0:T(8,128)(2,1)} %wv.1, bf16[32,512]{1,0:T(8,128)(2,1)} %bitcast.2, f32[4]{0:T(128)} %lam.1, f32[1,128]{1,0:T(1,128)} %bitcast.3), custom_call_target="tpu_custom_call" | custom-call | tf_op jit(solution)/shard_map/attention/pallas_call | solution.py:468
  90.5 2.0 %copy.9 = bf16[160,2048]{1,0:T(8,128)(2,1)} copy(bf16[160,2048]{1,0:T(8,128)(2,1)} %attention.1) | data formatting | bytes 1310720

commit v4 on v3

--- a/solution.py
+++ b/solution.py
@@ -17,6 +17,7 @@
 COLS = 2 * TOKS
 TILE = 256
 KINDS = 4
+W_KINDS = 8
 LOW = -1e30
 EXP_SCALE = 64 ** (-0.5) * math.log2(math.e)
 
@@ -28,7 +29,9 @@
 
 
 class ZRing:
-    def __init__(self, block, send, recv, sib_send):
+    def __init__(self, kinds, shared, pairs, block, send, recv, sib_send):
+        self.pairs = pairs
+        self.kinds, self.shared = kinds, shared
         self.block, self.send, self.recv, self.sib_send = block, send, recv, sib_send
         self.z, self.c = lax.axis_index("z"), lax.axis_index("core")
 
@@ -40,7 +43,8 @@
 
     def onward(self, way, d, kind, o):
         ref = self.block(o, self.c, kind)
-        to = lax.rem(self.z + (1 if way == 0 else NZ - 1), NZ)
+        reach = 2 - d % 2 if self.pairs else 1
+        to = lax.rem(self.z + (reach if way == 0 else NZ - reach), NZ)
         return rcopy(ref, ref, self.send.at[way, d - 1, kind], self.recv.at[o, self.c, kind], {"z": to})
 
     def share(self, o, kind):
@@ -51,37 +55,51 @@
         ref = self.block(o, c, kind)
         rcopy(ref, ref, self.sib_send.at[o, kind], self.recv.at[o, c, kind], {"core": 1 - self.c}).wait_recv()
 
-    def begin(self, kind):
-        for way in (0, 1):
-            self.onward(way, 1, kind, self.z).start()
-        self.share(self.z, kind).start()
+    def shares(self, kind):
+        return self.shared == self.kinds or kind < self.shared
+
+    def begin(self, kinds):
+        for d in (2, 1) if self.pairs else (1,):
+            for kind in kinds:
+                for way in (0, 1):
+                    self.onward(way, d, kind, self.z).start()
+        for kind in kinds:
+            if self.shares(kind):
+                self.share(self.z, kind).start()
 
     def pass_on(self, way, d, kind):
         o = self.origin(way, d)
         self.arrived(o, self.c, kind)
 
-        @pl.when(d < self.farthest(way, kind))
-        def _():
-            self.onward(way, d + 1, kind, o).start()
-
-        self.share(o, kind).start()
+        if self.pairs:
+            for far in range(3, self.farthest(way, kind) + 1) if d == 2 else ():
+                self.onward(way, far, kind, o).start()
+        else:
+
+            @pl.when(d < self.farthest(way, kind))
+            def _():
+                self.onward(way, d + 1, kind, o).start()
+
+        if self.shares(kind):
+            self.share(o, kind).start()
 
     def drain(self):
-        for kind in range(KINDS):
+        for kind in range(self.kinds):
             for way in (0, 1):
                 for d in range(1, self.farthest(way, kind) + 1):
                     self.onward(way, d, kind, self.z).wait_send()
 
-            @pl.loop(0, NZ)
-            def _(o):
-                self.share(o, kind).wait_send()
+            if self.shares(kind):
+                @pl.loop(0, NZ)
+                def _(o):
+                    self.share(o, kind).wait_send()
 
 
 def attention_kernel(
     tok, wq, wk, wv, wo, lam, gain, out,
     xbuf, wkv, wqs, kv, qrow, qbd, acc, top, wt, hrow, hbuf, osum,
     tok_s, tok_r, wy_s, wy_r, w_s, w_r, w_sib, kv_s, kv_r, kv_sib,
-    oz_s, oz_r, oy_s, oy_r, ox_s, of_s, ox_r, oc_s, oc_r, h_s, hf_s, h_r, hf_r,
+    o2_s, o2_r, o3_s, of_s, o3_r, oc_s, oc_r, h_s, hf_s, h_r, hf_r,
 ):
     z, y, c, x = (lax.axis_index(name) for name in ("z", "y", "core", "x"))
     right, left, facing = lax.rem(x + 1, NX), lax.rem(x + NX - 1, NX), lax.rem(x + 2, NX)
@@ -92,7 +110,7 @@
     friends = [{"y": lax.rem(y + k, NY)} for k in range(1, NY)]
     friends += [{"z": lax.rem(z + k, NZ)} for k in range(1, NZ)]
     friends += [{"y": lax.rem(y + k, NY), "x": to} for k in range(NY) for to in (left, right)]
-    friends += [{"core": 1 - c}]
+    friends += [{"x": facing}, {"core": 1 - c}]
     for friend in friends:
         pl.semaphore_signal(barrier, inc=1, device_id=friend, device_id_type=MESH)
     pl.semaphore_wait(barrier, len(friends))
@@ -133,58 +151,80 @@
     for copy in own:
         copy.start()
 
-    def piece(xx, yy):
-        return wt.at[xx, :, yy, c]
-
-    def half_piece(xx, yy, k):
-        return wt.at[xx, pl.ds(k * (NZ // 2), NZ // 2), yy, c]
-
-    def turn(i):
-        return lax.rem(y + jnp.where(i == 2, 3, jnp.where(i == 3, 2, i)), NY)
-
-    def o_z(k):
-        block = wt.at[x, z, y, c]
-        return rcopy(block, block, oz_s.at[k - 1], oz_r.at[z], {"z": lax.rem(z + k, NZ)})
-
-    def o_z_arrived(k):
-        frm = lax.rem(z + k, NZ)
-        block = wt.at[x, frm, y, c]
-        rcopy(block, block, oz_s.at[k - 1], oz_r.at[frm], {"z": frm}).wait_recv()
-
-    def o_y(k):
-        return rcopy(piece(x, y), piece(x, y), oy_s.at[k - 1], oy_r.at[y], {"y": lax.rem(y + k, NY)})
-
-    def o_y_arrived(yy):
-        rcopy(piece(x, yy), piece(x, yy), oy_s.at[0], oy_r.at[yy], {"y": above}).wait_recv()
-
-    def o_x(yy):
+    places = {"y": (y, above, below), "x": (x, right, left)}
+
+    def axes(h):
+        return ("y", "x") if h == 0 else ("x", "y")
+
+    def piece(h, a, b, core, z_half=None):
+        xx, yy = (b, a) if h == 0 else (a, b)
+        zs = slice(None) if z_half is None else pl.ds(z_half * (NZ // 2), NZ // 2)
+        return wt.at[h, xx, zs, yy, core]
+
+    def turn(i, at=y):
+        return lax.rem(at + jnp.where(i == 2, 3, jnp.where(i == 3, 2, i)), NY)
+
+    def o_second(h, k):
+        a, b = (places[name][0] for name in axes(h))
+        ref = piece(h, a, b, c)
+        return rcopy(ref, ref, o2_s.at[h, k - 1], o2_r.at[h, a], {axes(h)[0]: lax.rem(a + k, NY)})
+
+    def o_second_arrived(h, a):
+        ref = piece(h, a, places[axes(h)[1]][0], c)
+        rcopy(ref, ref, o2_s.at[h, 0], o2_r.at[h, a], {axes(h)[0]: places[axes(h)[0]][1]}).wait_recv()
+
+    def o_third(h, a):
+        name = axes(h)[1]
+        b, up, down = places[name]
         return [
-            rcopy(half_piece(x, yy, k), half_piece(x, yy, k), ox_s.at[yy, n], ox_r.at[x, yy, k], {"x": to})
-            for n, (k, to) in enumerate([(0, right), (1, left), (1, right), (0, left)])
+            rcopy(piece(h, a, b, c, k), piece(h, a, b, c, k), o3_s.at[h, a, n], o3_r.at[h, a, b, k], {name: to})
+            for n, (k, to) in enumerate([(0, up), (1, down), (1, up), (0, down)])
         ]
 
-    def o_x_arrived(xx, yy, k):
-        ref = half_piece(xx, yy, k)
-        rcopy(ref, ref, ox_s.at[yy, 0], ox_r.at[xx, yy, k], {"x": right}).wait_recv()
-
-    def o_relay(yy, k):
-        frm, to = ((left, right), (right, left))[k]
-        ref = half_piece(frm, yy, k)
-        return rcopy(ref, ref, of_s.at[yy, k], ox_r.at[frm, yy, k], {"x": to})
-
-    def o_share(xx, yy):
-        return rcopy(piece(xx, yy), piece(xx, yy), oc_s.at[xx, yy], oc_r.at[xx, yy], {"core": 1 - c})
-
-    def o_shared(xx, yy):
-        ref = wt.at[xx, :, yy, 1 - c]
-        rcopy(ref, ref, oc_s.at[xx, yy], oc_r.at[xx, yy], {"core": 1 - c}).wait_recv()
-
-    def o_spread(yy):
-        for copy in o_x(yy):
+    def o_third_arrived(h, a, b, k):
+        ref = piece(h, a, b, c, k)
+        name = axes(h)[1]
+        rcopy(ref, ref, o3_s.at[h, a, 0], o3_r.at[h, a, b, k], {name: places[name][1]}).wait_recv()
+
+    def o_relay(h, a, k):
+        name = axes(h)[1]
+        b, up, down = places[name]
+        frm, to = ((down, up), (up, down))[k]
+        ref = piece(h, a, frm, c, k)
+        return rcopy(ref, ref, of_s.at[h, a, k], o3_r.at[h, a, frm, k], {name: to})
+
+    def o_share(h, a, b):
+        ref = piece(h, a, b, c)
+        return rcopy(ref, ref, oc_s.at[h, a, b], oc_r.at[h, a, b], {"core": 1 - c})
+
+    def o_shared(h, a, b):
+        ref = piece(h, a, b, 1 - c)
+        rcopy(ref, ref, oc_s.at[h, a, b], oc_r.at[h, a, b], {"core": 1 - c}).wait_recv()
+
+    def o_spread(h, a):
+        for copy in o_third(h, a):
             copy.start()
-        o_share(x, yy).start()
-
-    wt[x, z, y, c] = wo[...]
+        o_share(h, a, places[axes(h)[1]][0]).start()
+
+    def w_block(o, cc, kind):
+        if kind < 4:
+            return wkv.at[o, kind, cc]
+        if kind < 6:
+            return wqs.at[o, pl.ds(2 * (kind - 4), 2), cc]
+        return wt.at[kind - 6, x, o, y, c]
+
+    w_ring = ZRing(W_KINDS, 6, True, w_block, w_s, w_r, w_sib)
+    ring = ZRing(KINDS, KINDS, False, lambda o, cc, kind: kv.at[o, cc, pl.ds(kind * ROWS, ROWS), :], kv_s, kv_r, kv_sib)
+
+    def pass_all(what, d, kinds):
+        for kind in kinds:
+            for way in (0, 1):
+                if d <= what.farthest(way, kind):
+                    what.pass_on(way, d, kind)
+
+    for h in (0, 1):
+        wt[h, x, z, y, c] = wo[:, h * wo.shape[1] // 2 : (h + 1) * wo.shape[1] // 2]
+    w_ring.begin((6, 7))
 
     mine = pl.ds(pl.multiple_of(y * HEAD, HEAD), HEAD)
     wqs[z, y, c] = wq[:, mine]
@@ -194,37 +234,26 @@
     acc[...] = jnp.zeros_like(acc)
     top[...] = jnp.full_like(top, LOW)
 
-    w_ring = ZRing(lambda o, cc, kind: (wkv, wqs)[kind // 2].at[o, pl.ds(2 * (kind % 2), 2), cc], w_s, w_r, w_sib)
-    ring = ZRing(lambda o, cc, kind: kv.at[o, cc, pl.ds(kind * ROWS, ROWS), :], kv_s, kv_r, kv_sib)
-
-    def pass_all(what, d, kinds):
-        for kind in kinds:
-            for way in (0, 1):
-                if d <= what.farthest(way, kind):
-                    what.pass_on(way, d, kind)
-
+    key_value, query, output = range(4), (4, 5), (6, 7)
     w_arrived(1)
     w_arrived(2)
-    for kind in (0, 1):
-        w_ring.begin(kind)
+    w_ring.begin(key_value)
+    pass_all(w_ring, 2, key_value)
+    pass_all(w_ring, 2, output)
     w_arrived(0)
-    for kind in (2, 3):
-        w_ring.begin(kind)
+    w_ring.begin(query)
     fwd_up = tok_copy(part(below, 0), below, 0, 4, above)
     fwd_down = tok_copy(part(above, 1), above, 1, 5, below)
-    for d in range(1, NZ // 2 + 1):
-        pass_all(w_ring, d, (0, 1))
-        if d > 1:
-            pass_all(w_ring, d - 1, (2, 3))
-        for k in {d, NZ - d}:
-            o_z(k).start()
-        if d == 2:
-            tok_arrived(below, 0)
-            fwd_up.start()
-            tok_arrived(above, 1)
-            fwd_down.start()
+    pass_all(w_ring, 1, key_value)
+    tok_arrived(below, 0)
+    fwd_up.start()
+    tok_arrived(above, 1)
+    fwd_down.start()
+    pass_all(w_ring, 2, query)
+    pass_all(w_ring, 3, key_value)
+    pass_all(w_ring, 4, key_value)
     for o in range(NZ):
-        for kind in (0, 1):
+        for kind in key_value:
             w_ring.arrived(o, 1 - c, kind)
 
     def project(i):
@@ -232,7 +261,7 @@
         kv[z, c, at, :] = jnp.dot(
             xbuf[turn(i)], wkv[...].reshape(-1, 2 * HEAD), preferred_element_type=jnp.float32
         ).astype(jnp.bfloat16)
-        ring.begin(i)
+        ring.begin((i,))
 
     def project_near(i, carry):
         @pl.when(i == 1)
@@ -248,19 +277,25 @@
 
     lax.fori_loop(0, NY - 1, project_near, 0)
 
-    pass_all(w_ring, NZ // 2, (2, 3))
-    for k in range(1, NZ):
-        o_z_arrived(k)
-    for k in range(1, NY):
-        o_y(k).start()
-    o_spread(y)
-    pass_all(ring, 1, range(NY - 1))
-    for o in range(NZ):
-        for kind in (2, 3):
-            w_ring.arrived(o, 1 - c, kind)
+    for d in (1, 3, 4):
+        pass_all(w_ring, d, output)
+    for h in (1, 0):
+        for k in (1, 3, 2):
+            o_second(h, k).start()
+        o_spread(h, places[axes(h)[0]][0])
+    for d in (1, 3, 4):
+        pass_all(w_ring, d, query)
+    for n in range(3):
+        for k in range(1, NY):
+            w_copy(k, n).wait_send()
+    w_ring.drain()
     for k in (0, 1):
         tok_arrived(across, k)
     project(NY - 1)
+    pass_all(ring, 1, range(NY - 1))
+    for o in range(NZ):
+        for kind in query:
+            w_ring.arrived(o, 1 - c, kind)
 
     def queries(i, carry):
         at = pl.ds(pl.multiple_of(i * ROWS, ROWS), ROWS)
@@ -347,20 +382,42 @@
 
                 lax.fori_loop(0, NC, both, 0)
 
-        @pl.when(d < NY)
+        @pl.when(d == 1)
         def _():
-            o_y_arrived(turn(d))
-            o_spread(turn(d))
-
-        @pl.when(d >= 2)
-        def _():
-            yy = turn(d - 2)
-            for k, frm in enumerate((left, right)):
-                o_x_arrived(frm, yy, k)
-                o_relay(yy, k).start()
-            for k, frm in enumerate((left, right)):
-                o_x_arrived(frm, yy, 1 - k)
-                o_share(frm, yy).start()
+            for k in (3, 1, 2):
+                for h in (1, 0):
+                    came = lax.rem(places[axes(h)[0]][0] + k, NY)
+                    o_second_arrived(h, came)
+                    o_spread(h, came)
+
+        def relay(i):
+            for h in (1, 0):
+                here, up, down = places[axes(h)[1]]
+                a = lax.rem(places[axes(h)[0]][0] + (0, 3, 1, 2)[i], NY)
+                for k, frm in enumerate((down, up)):
+                    o_third_arrived(h, a, frm, k)
+                    o_relay(h, a, k).start()
+                for k, frm in enumerate((down, up)):
+                    o_third_arrived(h, a, frm, 1 - k)
+                    o_share(h, a, frm).start()
+
+        def last(i):
+            for h in (1, 0):
+                a = lax.rem(places[axes(h)[0]][0] + (0, 3, 1, 2)[i], NY)
+                b = lax.rem(places[axes(h)[1]][0] + 2, NY)
+                for k in (0, 1):
+                    o_third_arrived(h, a, b, k)
+                o_share(h, a, b).start()
+
+        for i, at in enumerate((1, 2, 3, 3)):
+
+            @pl.when(d == at)
+            def _():
+                relay(i)
+
+            @pl.when(d == (4 if i < 2 else 5))
+            def _():
+                last(i)
 
         return carry
 
@@ -389,82 +446,75 @@
         ref = hbuf.at[frm, rows(k), :]
         return rcopy(ref, ref, hf_s.at[k], hf_r.at[k], {"x": to})
 
-    sent = []
+    sent = [h_copy(i, k, 4 + k, {}) for i in range(1, NY) for k in (0, 1)]
     for n, (k, to) in enumerate([(0, right), (1, left), (1, right), (0, left)]):
-        for i in range(NY):
-            sent.append(h_copy(i, k, n, {"x": to}))
-            sent[-1].start()
-        if n == 1:
-            for i in range(1, NY):
-                for kk in (0, 1):
-                    sent.append(h_copy(i, kk, 4 + kk, {}))
-                    sent[-1].start()
+        sent += [h_copy(i, k, n, {"x": to}) for i in range(NY)]
+    for copy in sent:
+        copy.start()
     hbuf[x, :, mine] = hrow[0]
+    for h in (0, 1):
+        for k in range(1, NY):
+            o_second(h, k).wait_send()
+        for a in range(NY):
+            for copy in o_third(h, a):
+                copy.wait_send()
+            for k in (0, 1):
+                o_relay(h, a, k).wait_send()
+            for b in range(NX):
+                o_share(h, a, b).wait_send()
+    for copy in own + [fwd_up, fwd_down]:
+        copy.wait_send()
+    ring.drain()
+    for i in range(1, NY):
+        for k in (0, 1):
+            h_arrived(x, lax.rem(y + i, NY), k)
+
+    depth = wt.shape[-1]
+
+    def weights_here(xx):
+        for h in (0, 1):
+            for yy in range(NY):
+                o_shared(h, *((yy, xx) if h == 0 else (xx, yy)))
+
+    def product(xx):
+        total = 0.0
+        for h in (0, 1):
+            total += lax.dot_general(
+                wt[h, xx].reshape(-1, depth),
+                hbuf[xx, :, h * depth : (h + 1) * depth],
+                (((1,), (1,)), ((), ())),
+                preferred_element_type=jnp.float32,
+            )
+        return total
+
+    for xx in range(NX):
+        weights_here(xx)
+    osum[...] = product(x)
     relays = [h_relay(0), h_relay(1)]
     for k, frm in enumerate((left, right)):
         for i in range(NY):
             h_arrived(frm, lax.rem(y + i, NY), k)
         relays[k].start()
-
-    for i in range(NY):
-        yy = turn(i)
-        for k in (0, 1):
-            o_x_arrived(facing, yy, k)
-        o_share(facing, yy).start()
-    for xx in (x, left, right):
-        for yy in range(NY):
-            o_shared(xx, yy)
-    for k in (0, 1):
-        for i in range(1, NY):
-            h_arrived(x, lax.rem(y + i, NY), k)
     for k, frm in enumerate((left, right)):
         for i in range(NY):
             h_arrived(frm, lax.rem(y + i, NY), 1 - k)
-
-    width = wo.shape[1]
-
-    def product(j, xx):
-        block = wt[xx, 2 * j : 2 * j + 2].reshape(width, width)
-        return lax.dot_general(block, hbuf[xx], (((1,), (1,)), ((), ())), preferred_element_type=jnp.float32)
-
-    for j in range(out.shape[1] // width):
-        osum[j] = product(j, x) + product(j, left) + product(j, right)
-    for yy in range(NY):
-        o_shared(facing, yy)
+    osum[...] += product(left) + product(right)
     for k in (0, 1):
         ref = hbuf.at[facing, rows(k), :]
         rcopy(ref, ref, hf_s.at[k], hf_r.at[k], {"x": right}).wait_recv()
-    for j in range(out.shape[1] // width):
-        out[:, j * width : (j + 1) * width] = (osum[j] + product(j, facing)).T.astype(jnp.bfloat16)
+    out[...] = (osum[...] + product(facing)).astype(jnp.bfloat16).T
 
     for copy in sent + relays:
         copy.wait_send()
-    for k in range(1, NZ):
-        o_z(k).wait_send()
-    for k in range(1, NY):
-        o_y(k).wait_send()
-    for yy in range(NY):
-        for copy in o_x(yy):
-            copy.wait_send()
-        for k in (0, 1):
-            o_relay(yy, k).wait_send()
-        for xx in range(NX):
-            o_share(xx, yy).wait_send()
-
-    for copy in own + [fwd_up, fwd_down]:
-        copy.wait_send()
-    for k in range(1, NY):
-        for n in range(3):
-            w_copy(k, n).wait_send()
-    w_ring.drain()
-    ring.drain()
 
 
 def attention(tokens, wq, wk, wv, wo, lam, gain):
     vmem = pl.BlockSpec(memory_space=pltpu.VMEM)
     dma = pltpu.SemaphoreType.DMA
     width = tokens.shape[1]
-    ring_sems = [dma((2, NZ // 2, KINDS)), dma((NZ, NC, KINDS)), dma((NZ, KINDS))]
+    w_sems, ring_sems = (
+        [dma((2, NZ // 2, kinds)), dma((NZ, NC, kinds)), dma((NZ, kinds))] for kinds in (W_KINDS, KINDS)
+    )
     return pl.pallas_call(
         attention_kernel,
         out_shape=jax.ShapeDtypeStruct(tokens.shape, jnp.bfloat16),
@@ -479,25 +529,23 @@
             pltpu.VMEM((HEAD, COLS), jnp.bfloat16),
             pltpu.VMEM((HEAD + 16, COLS), jnp.float32),
             pltpu.VMEM((8, COLS), jnp.float32),
-            pltpu.VMEM((NX, NZ, NY, NC, wo.shape[0], wo.shape[1]), jnp.bfloat16),
+            pltpu.VMEM((2, NX, NZ, NY, NC, wo.shape[0], wo.shape[1] // 2), jnp.bfloat16),
             pltpu.VMEM((NY, ROWS, HEAD), jnp.bfloat16),
             pltpu.VMEM((NX, ROWS, NY * HEAD), jnp.bfloat16),
-            pltpu.VMEM((width // wo.shape[1], wo.shape[1], ROWS), jnp.float32),
+            pltpu.VMEM((width, ROWS), jnp.float32),
             dma((6,)),
             dma((NY, 2)),
             dma((NY - 1, 3)),
             dma((NY, 3)),
+            *w_sems,
             *ring_sems,
-            *ring_sems,
-            dma((NZ - 1,)),
-            dma((NZ,)),
-            dma((NY - 1,)),
-            dma((NY,)),
-            dma((NY, 4)),
-            dma((NY, 2)),
-            dma((NX, NY, 2)),
-            dma((NX, NY)),
-            dma((NX, NY)),
+            dma((2, NY - 1)),
+            dma((2, NY)),
+            dma((2, NY, 4)),
+            dma((2, NY, 2)),
+            dma((2, NY, NX, 2)),
+            dma((2, NY, NX)),
+            dma((2, NY, NX)),
             dma((NY, 6)),
             dma((2,)),
             dma((NX, NY, 2)),

time: 92.6 us -> 82.8 us (0.89)
  the two profiles are of different devices: /device:TPU:4 before, /device:TPU:224 now
where the time goes in v4:
time: 82.8 us; the launch traced here: 82.7 us
  Pallas kernels  80.7 us (97%)
  local copies, waits for them, and re-layouts  1.98 us (2%)
    pallas_call x1, Pallas kernels, attention(): pl.pallas_call(attention_kernel, out_shape=jax.ShapeDtypeStruct(tokens.sh...  80.7 us
    unnamed x1, local copies, waits for them, and re-layouts  1.98 us

profile of v4, /device:TPU:224, one launch (start us, length us, event | category | flops | bytes accessed | tf_op | source)
XLA Modules:
  0.0 82.7 jit_solution(9579715886896733100)
XLA Ops:
  0.0 80.7 %attention.1 = bf16[160,2048]{1,0:T(8,128)(2,1)} custom-call(bf16[160,2048]{1,0:T(8,128)(2,1)} %tok.1, bf16[32,512]{1,0:T(8,128)(2,1)} %wq.1, bf16[32,512]{1,0:T(8,128)(2,1)} %wk.1, bf16[32,512]{1,0:T(8,128)(2,1)} %wv.1, bf16[32,512]{1,0:T(8,128)(2,1)} %bitcast.2, f32[4]{0:T(128)} %lam.1, f32[1,128]{1,0:T(1,128)} %bitcast.3), custom_call_target="tpu_custom_call" | custom-call | tf_op jit(solution)/shard_map/attention/pallas_call | solution.py:518
  80.7 2.0 %copy.9 = bf16[160,2048]{1,0:T(8,128)(2,1)} copy(bf16[160,2048]{1,0:T(8,128)(2,1)} %attention.1) | data formatting | bytes 1310720

commit v5 on v1

v5 whole, which is shorter than its diff:
```python
import functools
import math

import jax
import jax.numpy as jnp
from jax import lax
from jax.experimental import pallas as pl
from jax.experimental.pallas import tpu as pltpu
from jax.sharding import Mesh
from jax.sharding import PartitionSpec as P

MESH = pl.DeviceIdType.MESH
NZ, NY, NC, NX = 8, 4, 2, 4
ROWS = 160
TOKS = NY * ROWS
HEAD = 128
COLS = 2 * TOKS
TILE = 256
KINDS = 4
LOW = -1e30
EXP_SCALE = 64 ** (-0.5) * math.log2(math.e)


def rcopy(src, dst, send_sem, recv_sem, device):
    return pltpu.make_async_remote_copy(
        src_ref=src, dst_ref=dst, send_sem=send_sem, recv_sem=recv_sem, device_id=device, device_id_type=MESH
    )


def attention_kernel(
    tok, wq, wk, wv, wo, lam, gain, out,
    xbuf, wkv, wqs, kv, qrow, qbd, acc, top, wt, hrow, hbuf, osum,
    send, tok_r, wy_r, wkv_r, wqs_r, wo_r, w_sib, kv_r, kv_sib, o2_r, o3_r, oc_r, h_r,
):
    z, y, c, x = (lax.axis_index(name) for name in ("z", "y", "core", "x"))
    right, left, facing = lax.rem(x + 1, NX), lax.rem(x + NX - 1, NX), lax.rem(x + 2, NX)
    above, below = lax.rem(y + 1, NY), lax.rem(y + NY - 1, NY)
    across = lax.rem(y + 2, NY)

    barrier = pltpu.get_barrier_semaphore()
    friends = [{"y": lax.rem(y + k, NY)} for k in range(1, NY)]
    friends += [{"z": lax.rem(z + k, NZ)} for k in range(1, NZ)]
    friends += [{"y": lax.rem(y + k, NY), "x": to} for k in range(NY) for to in (left, right)]
    friends += [{"x": facing}, {"core": 1 - c}]
    for friend in friends:
        pl.semaphore_signal(barrier, inc=1, device_id=friend, device_id_type=MESH)
    pl.semaphore_wait(barrier, len(friends))

    half = ROWS // 2

    SEND_TOK, SEND_WY, SEND_W, SEND_KV, SEND_O, SEND_SHARE, SEND_H = range(7)

    def wide(rows):
        return kv.at[pl.ds(0, rows), :]

    def got(sem, ref):
        rcopy(ref, ref, send.at[0], sem, {"core": 1 - c}).wait_recv()

    def gone(group, ref):
        rcopy(ref, ref, send.at[group], oc_r.at[0], {"core": 1 - c}).wait_send()

    def part(slot, k):
        return xbuf.at[slot, pl.ds(k * half, half), :]

    def tok_copy(src, slot, k, n, to):
        rcopy(src, part(slot, k), send.at[SEND_TOK], tok_r.at[n], {"y": to}).start()

    def w_slot(frm, n):
        return (wqs.at[z, frm, c], wkv.at[z, frm, c, :, pl.ds(0, HEAD)], wkv.at[z, frm, c, :, pl.ds(HEAD, HEAD)])[n]

    for n in (1, 2, 0):
        for k in range(1, NY):
            to = lax.rem(y + k, NY)
            src = (wq, wk, wv)[n].at[:, pl.ds(pl.multiple_of(to * HEAD, HEAD), HEAD)]
            rcopy(src, w_slot(y, n), send.at[SEND_WY], wy_r.at[min(n, 1)], {"y": to}).start()
    first_half, second_half = tok.at[pl.ds(0, half), :], tok.at[pl.ds(half, half), :]
    tok_copy(first_half, y, 0, 0, above)
    tok_copy(second_half, y, 1, 1, below)
    tok_copy(second_half, y, 1, 2, above)
    tok_copy(first_half, y, 0, 3, below)

    places = {"y": (y, above, below), "x": (x, right, left)}

    def axes(h):
        return ("y", "x") if h == 0 else ("x", "y")

    def piece(h, a, b, core, z_half=None):
        xx, yy = (b, a) if h == 0 else (a, b)
        zs = slice(None) if z_half is None else pl.ds(z_half * (NZ // 2), NZ // 2)
        return wt.at[h, xx, zs, yy, core]

    def turn(i, at=y):
        return lax.rem(at + jnp.where(i == 2, 3, jnp.where(i == 3, 2, i)), NY)

    def o_second(h, k):
        a, b = (places[name][0] for name in axes(h))
        ref = piece(h, a, b, c)
        to = {axes(h)[0]: lax.rem(a + k, NY)}
        rcopy(ref, ref, send.at[SEND_O], o2_r.at[h, k - 1], to).start()

    def o_share(h, a, b):
        ref = piece(h, a, b, c)
        rcopy(ref, ref, send.at[SEND_SHARE], oc_r.at[0], {"core": 1 - c}).start()

    def o_a(h, i):
        return lax.rem(places[axes(h)[0]][0] + (0, 3, 1, 2)[i], NY)

    def o_third(h, i):
        name = axes(h)[1]
        b, up, down = places[name]
        for k, to, group in [(0, up, 0), (1, down, 0), (1, up, 1), (0, down, 1)]:
            ref = piece(h, o_a(h, i), b, c, k)
            rcopy(ref, ref, send.at[SEND_O], o3_r.at[i, group], {name: to}).start()
        o_share(h, o_a(h, i), b)

    def o_relay(i):
        got(o3_r.at[i, 0], wide(512))
        for h in (1, 0):
            name = axes(h)[1]
            b, up, down = places[name]
            for k, (frm, to) in enumerate(((down, up), (up, down))):
                ref = piece(h, o_a(h, i), frm, c, k)
                rcopy(ref, ref, send.at[SEND_O], o3_r.at[i, 2], {name: to}).start()
        got(o3_r.at[i, 1], wide(512))
        for h in (1, 0):
            for frm in places[axes(h)[1]][1:]:
                o_share(h, o_a(h, i), frm)

    def o_last(i):
        got(o3_r.at[i, 2], wide(512))
        for h in (1, 0):
            o_share(h, o_a(h, i), lax.rem(places[axes(h)[1]][0] + 2, NY))

    def origin(way, d):
        return lax.rem(z + (NZ - d if way == 0 else d), NZ)

    def z_copy(ref, way, reach, group, sem):
        to = lax.rem(z + (reach if way == 0 else NZ - reach), NZ)
        rcopy(ref, ref, send.at[group], sem, {"z": to}).start()

    def share(ref, group, sem):
        rcopy(ref, ref, send.at[group], sem, {"core": 1 - c}).start()

    class Weights:
        def __init__(self, block, sem, sib):
            self.block, self.sem, self.sib = block, sem, sib

        def begin(self):
            for d in (2, 1):
                for kind in (0, 1):
                    for way in (0, 1):
                        z_copy(self.block(z, kind), way, d, SEND_W, self.sem(way, d, kind))
            self.to_sibling(z, (0, 1))

        def to_sibling(self, o, kinds):
            if self.sib is not None:
                for kind in kinds:
                    share(self.block(o, kind), SEND_W, self.sib)

        def pass_on(self, way, kinds):
            o = origin(way, 2)
            for kind in kinds:
                z_copy(self.block(o, kind), way, 1, SEND_W, self.sem(way, 3, kind))
                if way == kind:
                    z_copy(self.block(o, kind), way, 2, SEND_W, self.sem(way, 4, kind))
            self.to_sibling(o, kinds)

        def arrived(self, d):
            for way in (0, 1):
                self.to_sibling(origin(way, d), (0, 1) if d < 4 else (way,))

    key_value = Weights(
        lambda o, kind: wkv.at[o, pl.ds(2 * kind, 2), c],
        lambda way, d, kind: wkv_r.at[2 * way + kind if d == 2 else {1: 4, 4: 5, 3: 6}[d]],
        w_sib.at[0],
    )
    query = Weights(
        lambda o, kind: wqs.at[o, pl.ds(2 * kind, 2), c],
        lambda way, d, kind: wqs_r.at[way if d == 2 else 2],
        w_sib.at[1],
    )
    output = Weights(
        lambda o, kind: wt.at[kind, x, o, y, c], lambda way, d, kind: wo_r.at[way if d == 2 else 2], None
    )

    def kv_block(o, cc, kind):
        return kv.at[pl.ds(pl.multiple_of(((o * NC + cc) * KINDS + kind) * ROWS, ROWS), ROWS), :]

    def farthest(way, kind):
        return NZ // 2 - (way != kind % 2)

    def kv_begin(kind):
        for way in (0, 1):
            z_copy(kv_block(z, c, kind), way, 1, SEND_KV, kv_r.at[way, 0, kind])
        share(kv_block(z, c, kind), SEND_KV, kv_sib.at[z])

    def kv_pass(way, d, kind):
        o = origin(way, d)
        got(kv_r.at[way, d - 1, kind], wide(ROWS))

        @pl.when(d < farthest(way, kind))
        def _():
            z_copy(kv_block(o, c, kind), way, 1, SEND_KV, kv_r.at[way, d, kind])

        share(kv_block(o, c, kind), SEND_KV, kv_sib.at[o])

    for h in (0, 1):
        wt[h, x, z, y, c] = wo[:, h * wo.shape[1] // 2 : (h + 1) * wo.shape[1] // 2]
    output.begin()

    mine = pl.ds(pl.multiple_of(y * HEAD, HEAD), HEAD)
    wqs[z, y, c] = wq[:, mine]
    wkv[z, y, c, :, :HEAD] = wk[:, mine]
    wkv[z, y, c, :, HEAD:] = wv[:, mine]
    xbuf[y] = tok[...]
    acc[...] = jnp.zeros_like(acc)
    top[...] = jnp.full_like(top, LOW)

    got(wy_r.at[1], wide(3 * 32))
    key_value.begin()
    for kind in (0, 1):
        for way in (0, 1):
            got(wkv_r.at[2 * way + kind], wide(64))
            key_value.pass_on(way, (kind,))
    for way in (0, 1):
        got(wo_r.at[way], wide(64))
        output.pass_on(way, (0, 1))
    got(wy_r.at[0], qrow.at[pl.ds(0, 3 * 32), :])
    query.begin()
    got(wkv_r.at[4], wide(256))
    key_value.arrived(1)
    got(tok_r.at[0], part(below, 0))
    tok_copy(part(below, 0), below, 0, 4, above)
    got(tok_r.at[1], part(above, 1))
    tok_copy(part(above, 1), above, 1, 4, below)
    for way in (0, 1):
        got(wqs_r.at[way], wide(64))
        query.pass_on(way, (0, 1))
    got(wkv_r.at[6], wide(256))
    key_value.arrived(3)
    got(wkv_r.at[5], wide(128))
    key_value.arrived(4)
    got(w_sib.at[0], wide(NZ * NY * 32))

    def project(i):
        kv_block(z, c, i)[...] = jnp.dot(
            xbuf[turn(i)], wkv[...].reshape(-1, 2 * HEAD), preferred_element_type=jnp.float32
        ).astype(jnp.bfloat16)
        kv_begin(i)

    def project_near(i, carry):
        @pl.when(i == 1)
        def _():
            got(tok_r.at[3], part(above, 0))

        @pl.when(i == 2)
        def _():
            got(tok_r.at[2], part(below, 1))

        project(i)
        return carry

    lax.fori_loop(0, NY - 1, project_near, 0)

    got(wo_r.at[2], wide(10 * 32))
    for h in (1, 0):
        for k in (1, 3, 2):
            o_second(h, k)
        o_third(h, 0)
    got(wqs_r.at[2], wide(10 * 32))
    for d in (1, 3, 4):
        query.arrived(d)
    gone(SEND_WY, qrow.at[pl.ds(0, 9 * 32), :])
    gone(SEND_W, wide(30 * 64 + 30 * 32 + 14 * 32))
    got(tok_r.at[4], xbuf.at[across])
    project(NY - 1)
    for kind in range(NY - 1):
        for way in (0, 1):
            kv_pass(way, 1, kind)
    got(w_sib.at[1], wide(NZ * NY * 16))

    def queries(i, carry):
        at = pl.ds(pl.multiple_of(i * ROWS, ROWS), ROWS)
        qrow[at, :] = jnp.dot(
            xbuf[turn(i)], wqs[...].reshape(-1, HEAD), preferred_element_type=jnp.float32
        ).astype(jnp.bfloat16)
        return carry

    lax.fori_loop(0, NY, queries, 0)
    q_t = qrow[...].T
    first = lax.broadcasted_iota(jnp.int32, q_t.shape, 0) < HEAD // 2
    zero = jnp.zeros_like(q_t)
    qbd[:, :TOKS] = jnp.where(first, q_t, zero)
    qbd[:, TOKS:] = jnp.where(first, zero, q_t)

    ones = jnp.ones((16, TOKS), jnp.bfloat16)

    def place(r, core):
        i = sum((r >= k * ROWS).astype(jnp.int32) for k in range(1, NY))
        return r + ROWS * (2 * turn(i) - i + core)

    def visit(o, cc, masked):
        at = pl.ds(pl.multiple_of((o * NC + cc) * TOKS, TOKS), TOKS)
        keys = kv[at, :HEAD]
        values = jnp.concatenate([kv[at, HEAD:].T, ones], axis=0)

        def scores(j):
            return jnp.dot(keys, qbd[:, j * TILE : (j + 1) * TILE], preferred_element_type=jnp.float32)

        ahead = scores(0)
        for j in range(COLS // TILE):
            cols = slice(j * TILE, (j + 1) * TILE)
            s = ahead
            if j + 1 < COLS // TILE:
                ahead = scores(j + 1)
            if masked:
                u = lax.broadcasted_iota(jnp.int32, (TOKS, 1), 0)
                t = lax.broadcasted_iota(jnp.int32, (1, TILE), 1) + j * TILE
                t = jnp.where(t >= TOKS, t - TOKS, t)
                s = jnp.where(place(u, cc) <= place(t, c), s, LOW)
            before = top[0:1, cols]
            now = jnp.maximum(before, jnp.max(s, axis=0, keepdims=True))
            shrink = jnp.exp2((before - now) * EXP_SCALE)
            p = jnp.exp2((s - now) * EXP_SCALE).astype(jnp.bfloat16)
            acc[:, cols] = acc[:, cols] * shrink + jnp.dot(values, p, preferred_element_type=jnp.float32)
            top[0:1, cols] = now

    def own_slice(k, carry):
        cc = jnp.where(k == 0, c, 1 - c)

        @pl.when(k == 1)
        def _():
            got(kv_sib.at[z], wide(TOKS))

        visit(z, cc, True)
        return carry

    lax.fori_loop(0, NC, own_slice, 0)

    def step(d, carry):
        for way in (0, 1):
            for kind in (2 * way, 2 * way + 1):
                for course in (0, 1):
                    due = d <= farthest(course, kind)

                    @pl.when(due if kind == KINDS - 1 else due & (d > 1))
                    def _():
                        kv_pass(course, d, kind)

            before = d - 1
            o = origin(way, before)
            there = (before >= 1) & (before <= NZ // 2 - way)

            @pl.when(there)
            def _():
                got(kv_sib.at[o], wide(TOKS))

            @pl.when(there & (o < z))
            def _():
                def both(cc, carry):
                    visit(o, cc, False)
                    return carry

                lax.fori_loop(0, NC, both, 0)

        @pl.when(d == 1)
        def _():
            for i, k in ((1, 1), (2, 3), (3, 2)):
                for h in (1, 0):
                    got(o2_r.at[h, k - 1], wide(256))
                    o_third(h, i)

        for i, at in enumerate((1, 2, 3, 3)):

            @pl.when(d == at)
            def _():
                o_relay(i)

            @pl.when(d == (4 if i < 2 else 5))
            def _():
                o_last(i)

        return carry

    lax.fori_loop(1, NZ // 2 + 2, step, 0)

    def part_of(cols):
        return acc[:HEAD, cols] / acc[HEAD : HEAD + 1, cols]

    mixture = part_of(slice(0, TOKS)) - lam[y] * part_of(slice(TOKS, COLS))
    scale = lax.rsqrt(jnp.mean(mixture * mixture, axis=0, keepdims=True) + 1e-05)
    hrow[...] = ((mixture * scale).T * gain[...]).astype(jnp.bfloat16).reshape(NY, ROWS, HEAD)

    def rows(k):
        return pl.ds(k * half, half)

    def h_copy(i, k, sem, device):
        dst = hbuf.at[x, rows(k), pl.ds(pl.multiple_of(y * HEAD, HEAD), HEAD)]
        rcopy(hrow.at[i, rows(k), :], dst, send.at[SEND_H], h_r.at[sem], {"y": turn(i), **device}).start()

    for i in range(1, NY):
        for k in (0, 1):
            h_copy(i, k, 0, {})
    for k, to, sem in [(0, right, 1), (1, left, 2), (1, right, 3), (0, left, 3)]:
        for i in range(NY):
            h_copy(i, k, sem, {"x": to})
    hbuf[x, :, mine] = hrow[0]
    gone(SEND_O, wide(6 * 256 + 48 * 128))
    gone(SEND_SHARE, wt.at[0])
    gone(SEND_TOK, xbuf.at[pl.ds(0, 3)])
    gone(SEND_KV, wide(60 * ROWS))
    got(h_r.at[0], wide(3 * half))

    depth = wt.shape[-1]

    def product(xx):
        total = 0.0
        for h in (0, 1):
            total += lax.dot_general(
                wt[h, xx].reshape(-1, depth),
                hbuf[xx, :, h * depth : (h + 1) * depth],
                (((1,), (1,)), ((), ())),
                preferred_element_type=jnp.float32,
            )
        return total

    got(oc_r.at[0], wt.at[0])
    osum[...] = product(x)
    for k, (frm, to) in enumerate(((left, right), (right, left))):
        got(h_r.at[1 + k], wide(2 * half))
        ref = hbuf.at[frm, rows(k), :]
        rcopy(ref, ref, send.at[SEND_H], h_r.at[4], {"x": to}).start()
    got(h_r.at[3], wide(4 * half))
    osum[...] += product(left) + product(right)
    got(h_r.at[4], wide(4 * half))
    out[...] = (osum[...] + product(facing)).astype(jnp.bfloat16).T

    gone(SEND_H, wide(22 * half // 2 + 4 * half))


def attention(tokens, wq, wk, wv, wo, lam, gain):
    vmem = pl.BlockSpec(memory_space=pltpu.VMEM)
    dma = pltpu.SemaphoreType.DMA
    width = tokens.shape[1]
    return pl.pallas_call(
        attention_kernel,
        out_shape=jax.ShapeDtypeStruct(tokens.shape, jnp.bfloat16),
        in_specs=[vmem, vmem, vmem, vmem, vmem, pl.BlockSpec(memory_space=pltpu.SMEM), vmem],
        out_specs=vmem,
        scratch_shapes=[
            pltpu.VMEM((NY, ROWS, width), jnp.bfloat16),
            pltpu.VMEM((NZ, NY, NC, wq.shape[0], 2 * HEAD), jnp.bfloat16),
            pltpu.VMEM((NZ, NY, NC, wq.shape[0], HEAD), jnp.bfloat16),
            pltpu.VMEM((NZ * NC * TOKS, 2 * HEAD), jnp.bfloat16),
            pltpu.VMEM((TOKS, HEAD), jnp.bfloat16),
            pltpu.VMEM((HEAD, COLS), jnp.bfloat16),
            pltpu.VMEM((HEAD + 16, COLS), jnp.float32),
            pltpu.VMEM((8, COLS), jnp.float32),
            pltpu.VMEM((2, NX, NZ, NY, NC, wo.shape[0], wo.shape[1] // 2), jnp.bfloat16),
            pltpu.VMEM((NY, ROWS, HEAD), jnp.bfloat16),
            pltpu.VMEM((NX, ROWS, NY * HEAD), jnp.bfloat16),
            pltpu.VMEM((width, ROWS), jnp.float32),
            dma((7,)),
            dma((5,)),
            dma((2,)),
            dma((7,)),
            dma((3,)),
            dma((3,)),
            dma((2,)),
            dma((2, NZ // 2, KINDS)),
            dma((NZ,)),
            dma((2, NY - 1)),
            dma((NY, 3)),
            dma((1,)),
            dma((5,)),
        ],
        compiler_params=pltpu.CompilerParams(
            collective_id=0, has_side_effects=True, vmem_limit_bytes=56 * 1024 * 1024
        ),
        name="attention",
    )(tokens, wq, wk, wv, wo, lam, gain.reshape(1, -1))


def on_device(tokens, query_weight, key_weight, value_weight, out_weight, mix_lambda, head_gain):
    return attention(tokens, query_weight, key_weight, value_weight, out_weight.T, mix_lambda, head_gain)


def solution(mesh):
    fine = Mesh(mesh.devices.reshape(NZ, NY, NC, NX), ("z", "y", "core", "x"))
    sp = ("z", "y", "core")
    placed = (P(sp, None), P(sp, "x"), P(sp, "x"), P(sp, "x"), P("x", sp), P("x"), P())
    return jax.shard_map(on_device, mesh=fine, in_specs=placed, out_specs=P(sp, None), check_vma=False)
```

time: 149 us -> 77.8 us (0.52); the launches traced: 146 us -> 77.7 us
  blocking collectives: 22.7 us -> 0 us
  waiting for transfers between devices: 22.5 us -> 0 us
  between operations: 13.4 us -> 0.01 us
  Pallas kernels: 81.8 us -> 75.7 us
  matrix products: 3.26 us -> 0 us
    reduce_scatter x1 -> x0, waiting for transfers between devices: 21.8 us -> none  [on_device(): lax.psum_scatter(partial_out.astype(jnp.bfloat16), 'x', scatter_dimension...]
    all_gather x1 -> x0, blocking collectives: 13.2 us -> none  [on_device(): return lax.all_gather(own, 'x', axis=0, tiled=True)]
    all_to_all x1 -> x0, blocking collectives: 9.48 us -> none  [on_device(): mine = lax.all_to_all(head_out.reshape(NY, ROWS, HEAD), 'y', 0, 0)]
    pallas_call x1, Pallas kernels: 81.8 us -> 75.7 us  [attention(): pl.pallas_call(attention_kernel, out_shape=jax.ShapeDtypeStruct(tokens.sh...]
    dot_general x1 -> x0, matrix products: 3.26 us -> none  [on_device(): lax.dot_general(mine, out_t, (((1,), (1,)), ((), ())), preferred_element_...]
  transfers between devices with their start and end apart: 2 -> 0, of which waited for: 1 -> 0; matrix products, arithmetic and copies ran while one was open for 1% -> 0% of each run, Pallas kernels for 56% -> 0%
where the time goes in v5:
time: 77.8 us; the launch traced here: 77.7 us
  Pallas kernels  75.7 us (97%)
  local copies, waits for them, and re-layouts  1.98 us (3%)
    pallas_call x1, Pallas kernels, attention(): pl.pallas_call(attention_kernel, out_shape=jax.ShapeDtypeStruct(tokens.sh...  75.7 us
    unnamed x1, local copies, waits for them, and re-layouts  1.98 us

profile of v5, /device:TPU:224, one launch (start us, length us, event | category | flops | bytes accessed | tf_op | source)
XLA Modules:
  0.0 77.7 jit_solution(9398502365808476581)
XLA Ops:
  0.0 75.7 %attention.1 = bf16[160,2048]{1,0:T(8,128)(2,1)} custom-call(bf16[160,2048]{1,0:T(8,128)(2,1)} %tok.1, bf16[32,512]{1,0:T(8,128)(2,1)} %wq.1, bf16[32,512]{1,0:T(8,128)(2,1)} %wk.1, bf16[32,512]{1,0:T(8,128)(2,1)} %wv.1, bf16[32,512]{1,0:T(8,128)(2,1)} %bitcast.2, f32[4]{0:T(128)} %lam.1, f32[1,128]{1,0:T(1,128)} %bitcast.3), custom_call_target="tpu_custom_call" | custom-call | tf_op jit(solution)/shard_map/attention/pallas_call | solution.py:445
  75.7 2.0 %copy.9 = bf16[160,2048]{1,0:T(8,128)(2,1)} copy(bf16[160,2048]{1,0:T(8,128)(2,1)} %attention.1) | data formatting | bytes 1310720

commit v6 on v5

--- a/solution.py
+++ b/solution.py
@@ -29,13 +29,22 @@
 
 def attention_kernel(
     tok, wq, wk, wv, wo, lam, gain, out,
-    xbuf, wkv, wqs, kv, qrow, qbd, acc, top, wt, hrow, hbuf, osum,
-    send, tok_r, wy_r, wkv_r, wqs_r, wo_r, w_sib, kv_r, kv_sib, o2_r, o3_r, oc_r, h_r,
+    xbuf, wloc, wkv, wqs, kv, qrow, qbd, acc, top, wt, hrow, hbuf, osum,
+    into, send, tok_r, wy_r, wkv_r, wqs_r, wo_r, w_sib, kv_r, kv_sib, o2_r, o3_r, oc_r, h_r,
 ):
     z, y, c, x = (lax.axis_index(name) for name in ("z", "y", "core", "x"))
     right, left, facing = lax.rem(x + 1, NX), lax.rem(x + NX - 1, NX), lax.rem(x + 2, NX)
     above, below = lax.rem(y + 1, NY), lax.rem(y + NY - 1, NY)
     across = lax.rem(y + 2, NY)
+
+    inputs = [
+        pltpu.make_async_copy(src, dst, into.at[n])
+        for n, (src, dst) in enumerate(
+            [(wk, wloc.at[1]), (wv, wloc.at[2]), (wq, wloc.at[0]), (tok, xbuf.at[y]), (wo, wt.at[x, z, y, c])]
+        )
+    ]
+    for copy in inputs:
+        copy.start()
 
     barrier = pltpu.get_barrier_semaphore()
     friends = [{"y": lax.rem(y + k, NY)} for k in range(1, NY)]
@@ -44,6 +53,8 @@
     friends += [{"x": facing}, {"core": 1 - c}]
     for friend in friends:
         pl.semaphore_signal(barrier, inc=1, device_id=friend, device_id_type=MESH)
+    for copy in inputs:
+        copy.wait()
     pl.semaphore_wait(barrier, len(friends))
 
     half = ROWS // 2
@@ -59,11 +70,22 @@
     def gone(group, ref):
         rcopy(ref, ref, send.at[group], oc_r.at[0], {"core": 1 - c}).wait_send()
 
-    def part(slot, k):
-        return xbuf.at[slot, pl.ds(k * half, half), :]
-
-    def tok_copy(src, slot, k, n, to):
-        rcopy(src, part(slot, k), send.at[SEND_TOK], tok_r.at[n], {"y": to}).start()
+    share_of = xbuf.shape[2] // 4
+    near = pl.ds(pl.multiple_of(lax.rem(x, 2) * share_of, share_of), 3 * share_of)
+    missed = pl.ds(pl.multiple_of(lax.rem(x, 2) * 3 * share_of, share_of), share_of)
+
+    def part(slot, k, lanes=near):
+        return xbuf.at[slot, pl.ds(k * half, half), lanes]
+
+    def tok_copy(slot, k, n, to):
+        rcopy(part(slot, k), part(slot, k), send.at[SEND_TOK], tok_r.at[n], {"y": to}).start()
+
+    def tok_aside(slot, k, n):
+        ref = part(slot, k, missed)
+        rcopy(ref, ref, send.at[SEND_TOK], tok_r.at[n], {"x": (right, left)[k]}).start()
+
+    def tok_complete(slot, n):
+        got(tok_r.at[n], xbuf.at[slot, :, pl.ds(0, share_of)])
 
     def w_slot(frm, n):
         return (wqs.at[z, frm, c], wkv.at[z, frm, c, :, pl.ds(0, HEAD)], wkv.at[z, frm, c, :, pl.ds(HEAD, HEAD)])[n]
@@ -71,14 +93,14 @@
     for n in (1, 2, 0):
         for k in range(1, NY):
             to = lax.rem(y + k, NY)
-            src = (wq, wk, wv)[n].at[:, pl.ds(pl.multiple_of(to * HEAD, HEAD), HEAD)]
+            src = wloc.at[n, :, pl.ds(pl.multiple_of(to * HEAD, HEAD), HEAD)]
             rcopy(src, w_slot(y, n), send.at[SEND_WY], wy_r.at[min(n, 1)], {"y": to}).start()
-    first_half, second_half = tok.at[pl.ds(0, half), :], tok.at[pl.ds(half, half), :]
-    tok_copy(first_half, y, 0, 0, above)
-    tok_copy(second_half, y, 1, 1, below)
-    tok_copy(second_half, y, 1, 2, above)
-    tok_copy(first_half, y, 0, 3, below)
-
+    tok_copy(y, 0, 0, above)
+    tok_copy(y, 1, 1, below)
+    tok_copy(y, 1, 2, above)
+    tok_copy(y, 0, 3, below)
+
+    depth = wo.shape[1] // 2
     places = {"y": (y, above, below), "x": (x, right, left)}
 
     def axes(h):
@@ -87,7 +109,7 @@
     def piece(h, a, b, core, z_half=None):
         xx, yy = (b, a) if h == 0 else (a, b)
         zs = slice(None) if z_half is None else pl.ds(z_half * (NZ // 2), NZ // 2)
-        return wt.at[h, xx, zs, yy, core]
+        return wt.at[xx, zs, yy, core, :, pl.ds(h * depth, depth)]
 
     def turn(i, at=y):
         return lax.rem(at + jnp.where(i == 2, 3, jnp.where(i == 3, 2, i)), NY)
@@ -180,7 +202,7 @@
         w_sib.at[1],
     )
     output = Weights(
-        lambda o, kind: wt.at[kind, x, o, y, c], lambda way, d, kind: wo_r.at[way if d == 2 else 2], None
+        lambda o, kind: wt.at[x, o, y, c, :, pl.ds(kind * depth, depth)], lambda way, d, kind: wo_r.at[way if d == 2 else 2], None
     )
 
     def kv_block(o, cc, kind):
@@ -204,15 +226,12 @@
 
         share(kv_block(o, c, kind), SEND_KV, kv_sib.at[o])
 
-    for h in (0, 1):
-        wt[h, x, z, y, c] = wo[:, h * wo.shape[1] // 2 : (h + 1) * wo.shape[1] // 2]
     output.begin()
 
     mine = pl.ds(pl.multiple_of(y * HEAD, HEAD), HEAD)
-    wqs[z, y, c] = wq[:, mine]
-    wkv[z, y, c, :, :HEAD] = wk[:, mine]
-    wkv[z, y, c, :, HEAD:] = wv[:, mine]
-    xbuf[y] = tok[...]
+    wqs[z, y, c] = wloc[0, :, mine]
+    wkv[z, y, c, :, :HEAD] = wloc[1, :, mine]
+    wkv[z, y, c, :, HEAD:] = wloc[2, :, mine]
     acc[...] = jnp.zeros_like(acc)
     top[...] = jnp.full_like(top, LOW)
 
@@ -230,16 +249,22 @@
     got(wkv_r.at[4], wide(256))
     key_value.arrived(1)
     got(tok_r.at[0], part(below, 0))
-    tok_copy(part(below, 0), below, 0, 4, above)
+    tok_copy(below, 0, 4, above)
+    tok_aside(below, 0, 6)
     got(tok_r.at[1], part(above, 1))
-    tok_copy(part(above, 1), above, 1, 4, below)
-    for way in (0, 1):
-        got(wqs_r.at[way], wide(64))
-        query.pass_on(way, (0, 1))
+    tok_copy(above, 1, 4, below)
+    tok_aside(above, 1, 5)
     got(wkv_r.at[6], wide(256))
     key_value.arrived(3)
     got(wkv_r.at[5], wide(128))
     key_value.arrived(4)
+    for way in (0, 1):
+        got(wqs_r.at[way], wide(64))
+        query.pass_on(way, (0, 1))
+    got(tok_r.at[2], part(below, 1))
+    tok_aside(below, 1, 6)
+    got(tok_r.at[3], part(above, 0))
+    tok_aside(above, 0, 5)
     got(w_sib.at[0], wide(NZ * NY * 32))
 
     def project(i):
@@ -251,17 +276,20 @@
     def project_near(i, carry):
         @pl.when(i == 1)
         def _():
-            got(tok_r.at[3], part(above, 0))
+            tok_complete(above, 5)
 
         @pl.when(i == 2)
         def _():
-            got(tok_r.at[2], part(below, 1))
+            tok_complete(below, 6)
 
         project(i)
         return carry
 
     lax.fori_loop(0, NY - 1, project_near, 0)
 
+    got(tok_r.at[4], xbuf.at[across, :, near])
+    for k in (0, 1):
+        tok_aside(across, k, 7)
     got(wo_r.at[2], wide(10 * 32))
     for h in (1, 0):
         for k in (1, 3, 2):
@@ -272,7 +300,7 @@
         query.arrived(d)
     gone(SEND_WY, qrow.at[pl.ds(0, 9 * 32), :])
     gone(SEND_W, wide(30 * 64 + 30 * 32 + 14 * 32))
-    got(tok_r.at[4], xbuf.at[across])
+    tok_complete(across, 7)
     project(NY - 1)
     for kind in range(NY - 1):
         for way in (0, 1):
@@ -293,14 +321,14 @@
     qbd[:, :TOKS] = jnp.where(first, q_t, zero)
     qbd[:, TOKS:] = jnp.where(first, zero, q_t)
 
-    ones = jnp.ones((16, TOKS), jnp.bfloat16)
+    ones = jnp.ones((16, NC * TOKS), jnp.bfloat16)
 
     def place(r, core):
         i = sum((r >= k * ROWS).astype(jnp.int32) for k in range(1, NY))
         return r + ROWS * (2 * turn(i) - i + core)
 
-    def visit(o, cc, masked):
-        at = pl.ds(pl.multiple_of((o * NC + cc) * TOKS, TOKS), TOKS)
+    def visit(o, masked):
+        at = pl.ds(pl.multiple_of(o * NC * TOKS, NC * TOKS), NC * TOKS)
         keys = kv[at, :HEAD]
         values = jnp.concatenate([kv[at, HEAD:].T, ones], axis=0)
 
@@ -314,10 +342,11 @@
             if j + 1 < COLS // TILE:
                 ahead = scores(j + 1)
             if masked:
-                u = lax.broadcasted_iota(jnp.int32, (TOKS, 1), 0)
+                u = lax.broadcasted_iota(jnp.int32, (NC * TOKS, 1), 0)
+                core = (u >= TOKS).astype(jnp.int32)
                 t = lax.broadcasted_iota(jnp.int32, (1, TILE), 1) + j * TILE
                 t = jnp.where(t >= TOKS, t - TOKS, t)
-                s = jnp.where(place(u, cc) <= place(t, c), s, LOW)
+                s = jnp.where(place(u - TOKS * core, core) <= place(t, c), s, LOW)
             before = top[0:1, cols]
             now = jnp.maximum(before, jnp.max(s, axis=0, keepdims=True))
             shrink = jnp.exp2((before - now) * EXP_SCALE)
@@ -325,17 +354,13 @@
             acc[:, cols] = acc[:, cols] * shrink + jnp.dot(values, p, preferred_element_type=jnp.float32)
             top[0:1, cols] = now
 
-    def own_slice(k, carry):
-        cc = jnp.where(k == 0, c, 1 - c)
-
-        @pl.when(k == 1)
-        def _():
-            got(kv_sib.at[z], wide(TOKS))
-
-        visit(z, cc, True)
-        return carry
-
-    lax.fori_loop(0, NC, own_slice, 0)
+    got(kv_sib.at[z], wide(TOKS))
+    visit(z, True)
+
+    def pieces_on(h):
+        for i, k in ((1, 1), (2, 3), (3, 2)):
+            got(o2_r.at[h, k - 1], wide(256))
+            o_third(h, i)
 
     def step(d, carry):
         for way in (0, 1):
@@ -357,28 +382,23 @@
 
             @pl.when(there & (o < z))
             def _():
-                def both(cc, carry):
-                    visit(o, cc, False)
-                    return carry
-
-                lax.fori_loop(0, NC, both, 0)
+                visit(o, False)
+
+            if way == 0:
+
+                @pl.when(d == 2)
+                def _():
+                    pieces_on(0)
 
         @pl.when(d == 1)
         def _():
-            for i, k in ((1, 1), (2, 3), (3, 2)):
-                for h in (1, 0):
-                    got(o2_r.at[h, k - 1], wide(256))
-                    o_third(h, i)
-
-        for i, at in enumerate((1, 2, 3, 3)):
+            pieces_on(1)
+
+        for i, at in enumerate((2, 3, 4, 4)):
 
             @pl.when(d == at)
             def _():
                 o_relay(i)
-
-            @pl.when(d == (4 if i < 2 else 5))
-            def _():
-                o_last(i)
 
         return carry
 
@@ -405,31 +425,28 @@
         for i in range(NY):
             h_copy(i, k, sem, {"x": to})
     hbuf[x, :, mine] = hrow[0]
-    gone(SEND_O, wide(6 * 256 + 48 * 128))
-    gone(SEND_SHARE, wt.at[0])
-    gone(SEND_TOK, xbuf.at[pl.ds(0, 3)])
-    gone(SEND_KV, wide(60 * ROWS))
-    got(h_r.at[0], wide(3 * half))
-
-    depth = wt.shape[-1]
-
-    def product(xx):
-        total = 0.0
-        for h in (0, 1):
-            total += lax.dot_general(
-                wt[h, xx].reshape(-1, depth),
-                hbuf[xx, :, h * depth : (h + 1) * depth],
-                (((1,), (1,)), ((), ())),
-                preferred_element_type=jnp.float32,
-            )
-        return total
-
-    got(oc_r.at[0], wt.at[0])
-    osum[...] = product(x)
+    for i in range(NY):
+        o_last(i)
     for k, (frm, to) in enumerate(((left, right), (right, left))):
         got(h_r.at[1 + k], wide(2 * half))
         ref = hbuf.at[frm, rows(k), :]
         rcopy(ref, ref, send.at[SEND_H], h_r.at[4], {"x": to}).start()
+    got(h_r.at[0], wide(3 * half))
+
+    def product(xx):
+        return lax.dot_general(
+            wt[xx].reshape(-1, wo.shape[1]),
+            hbuf[xx],
+            (((1,), (1,)), ((), ())),
+            preferred_element_type=jnp.float32,
+        )
+
+    got(oc_r.at[0], wt.at[pl.ds(0, 2)])
+    osum[...] = product(x)
+    gone(SEND_O, wide(6 * 256 + 48 * 128))
+    gone(SEND_SHARE, wt.at[pl.ds(0, 2)])
+    gone(SEND_TOK, xbuf.at[pl.ds(0, 3)])
+    gone(SEND_KV, wide(60 * ROWS))
     got(h_r.at[3], wide(4 * half))
     osum[...] += product(left) + product(right)
     got(h_r.at[4], wide(4 * half))
@@ -440,15 +457,17 @@
 
 def attention(tokens, wq, wk, wv, wo, lam, gain):
     vmem = pl.BlockSpec(memory_space=pltpu.VMEM)
+    hbm = pl.BlockSpec(memory_space=pltpu.HBM)
     dma = pltpu.SemaphoreType.DMA
     width = tokens.shape[1]
     return pl.pallas_call(
         attention_kernel,
         out_shape=jax.ShapeDtypeStruct(tokens.shape, jnp.bfloat16),
-        in_specs=[vmem, vmem, vmem, vmem, vmem, pl.BlockSpec(memory_space=pltpu.SMEM), vmem],
+        in_specs=[hbm, hbm, hbm, hbm, hbm, pl.BlockSpec(memory_space=pltpu.SMEM), vmem],
         out_specs=vmem,
         scratch_shapes=[
             pltpu.VMEM((NY, ROWS, width), jnp.bfloat16),
+            pltpu.VMEM((3, *wq.shape), jnp.bfloat16),
             pltpu.VMEM((NZ, NY, NC, wq.shape[0], 2 * HEAD), jnp.bfloat16),
             pltpu.VMEM((NZ, NY, NC, wq.shape[0], HEAD), jnp.bfloat16),
             pltpu.VMEM((NZ * NC * TOKS, 2 * HEAD), jnp.bfloat16),
@@ -456,12 +475,13 @@
             pltpu.VMEM((HEAD, COLS), jnp.bfloat16),
             pltpu.VMEM((HEAD + 16, COLS), jnp.float32),
             pltpu.VMEM((8, COLS), jnp.float32),
-            pltpu.VMEM((2, NX, NZ, NY, NC, wo.shape[0], wo.shape[1] // 2), jnp.bfloat16),
+            pltpu.VMEM((NX, NZ, NY, NC, wo.shape[0], wo.shape[1]), jnp.bfloat16),
             pltpu.VMEM((NY, ROWS, HEAD), jnp.bfloat16),
             pltpu.VMEM((NX, ROWS, NY * HEAD), jnp.bfloat16),
             pltpu.VMEM((width, ROWS), jnp.float32),
+            dma((5,)),
             dma((7,)),
-            dma((5,)),
+            dma((8,)),
             dma((2,)),
             dma((7,)),
             dma((3,)),

time: 77.8 us -> 75 us (0.964)
  Pallas kernels: 75.7 us -> 72.8 us
    pallas_call x1, Pallas kernels: 75.7 us -> 72.8 us  [attention(): pl.pallas_call(attention_kernel, out_shape=jax.ShapeDtypeStruct(tokens.sh...]
where the time goes in v6:
time: 75 us; the launch traced here: 74.8 us
  Pallas kernels  72.8 us (97%)
  local copies, waits for them, and re-layouts  1.98 us (3%)
    pallas_call x1, Pallas kernels, attention(): pl.pallas_call(attention_kernel, out_shape=jax.ShapeDtypeStruct(tokens.sh...  72.8 us
    unnamed x1, local copies, waits for them, and re-layouts  1.98 us

profile of v6, /device:TPU:224, one launch (start us, length us, event | category | flops | bytes accessed | tf_op | source)
XLA Modules:
  0.0 74.8 jit_solution(13837295172242032674)
XLA Ops:
  0.0 72.8 %attention.1 = bf16[160,2048]{1,0:T(8,128)(2,1)} custom-call(bf16[160,2048]{1,0:T(8,128)(2,1)} %tok.1, bf16[32,512]{1,0:T(8,128)(2,1)} %wq.1, bf16[32,512]{1,0:T(8,128)(2,1)} %wk.1, bf16[32,512]{1,0:T(8,128)(2,1)} %wv.1, bf16[32,512]{1,0:T(8,128)(2,1)} %bitcast.2, f32[4]{0:T(128)} %lam.1, f32[1,128]{1,0:T(1,128)} %bitcast.3), custom_call_target="tpu_custom_call" | custom-call | tf_op jit(solution)/shard_map/attention/pallas_call | solution.py:463
  72.8 2.0 %copy.9 = bf16[160,2048]{1,0:T(8,128)(2,1)} copy(bf16[160,2048]{1,0:T(8,128)(2,1)} %attention.1) | data formatting | bytes 1310720

commit v7 on v6

--- a/solution.py
+++ b/solution.py
@@ -435,8 +435,8 @@
 
     def product(xx):
         return lax.dot_general(
+            hbuf[xx],
             wt[xx].reshape(-1, wo.shape[1]),
-            hbuf[xx],
             (((1,), (1,)), ((), ())),
             preferred_element_type=jnp.float32,
         )
@@ -450,7 +450,7 @@
     got(h_r.at[3], wide(4 * half))
     osum[...] += product(left) + product(right)
     got(h_r.at[4], wide(4 * half))
-    out[...] = (osum[...] + product(facing)).astype(jnp.bfloat16).T
+    out[...] = (osum[...] + product(facing)).astype(jnp.bfloat16)
 
     gone(SEND_H, wide(22 * half // 2 + 4 * half))
 
@@ -478,7 +478,7 @@
             pltpu.VMEM((NX, NZ, NY, NC, wo.shape[0], wo.shape[1]), jnp.bfloat16),
             pltpu.VMEM((NY, ROWS, HEAD), jnp.bfloat16),
             pltpu.VMEM((NX, ROWS, NY * HEAD), jnp.bfloat16),
-            pltpu.VMEM((width, ROWS), jnp.float32),
+            pltpu.VMEM((ROWS, width), jnp.float32),
             dma((5,)),
             dma((7,)),
             dma((8,)),

time: 75 us -> 73.8 us (0.984)
  Pallas kernels: 72.8 us -> 70.9 us
    pallas_call x1, Pallas kernels: 72.8 us -> 70.9 us  [attention(): pl.pallas_call(attention_kernel, out_shape=jax.ShapeDtypeStruct(tokens.sh...]
where the time goes in v7:
time: 73.8 us; the launch traced here: 72.9 us
  Pallas kernels  70.9 us (96%)
  local copies, waits for them, and re-layouts  1.98 us (3%)
    pallas_call x1, Pallas kernels, attention(): pl.pallas_call(attention_kernel, out_shape=jax.ShapeDtypeStruct(tokens.sh...  70.9 us
    unnamed x1, local copies, waits for them, and re-layouts  1.98 us

profile of v7, /device:TPU:224, one launch (start us, length us, event | category | flops | bytes accessed | tf_op | source)
XLA Modules:
  0.0 72.9 jit_solution(17987511345214239189)
XLA Ops:
  0.0 70.9 %attention.1 = bf16[160,2048]{1,0:T(8,128)(2,1)} custom-call(bf16[160,2048]{1,0:T(8,128)(2,1)} %tok.1, bf16[32,512]{1,0:T(8,128)(2,1)} %wq.1, bf16[32,512]{1,0:T(8,128)(2,1)} %wk.1, bf16[32,512]{1,0:T(8,128)(2,1)} %wv.1, bf16[32,512]{1,0:T(8,128)(2,1)} %bitcast.2, f32[4]{0:T(128)} %lam.1, f32[1,128]{1,0:T(1,128)} %bitcast.3), custom_call_target="tpu_custom_call" | custom-call | tf_op jit(solution)/shard_map/attention/pallas_call | solution.py:463
  70.9 2.0 %copy.9 = bf16[160,2048]{1,0:T(8,128)(2,1)} copy(bf16[160,2048]{1,0:T(8,128)(2,1)} %attention.1) | data formatting | bytes 1310720

commit v8 on v7

--- a/solution.py
+++ b/solution.py
@@ -300,9 +300,11 @@
         query.arrived(d)
     gone(SEND_WY, qrow.at[pl.ds(0, 9 * 32), :])
     gone(SEND_W, wide(30 * 64 + 30 * 32 + 14 * 32))
+    for way in (0, 1):
+        kv_pass(way, 1, 0)
     tok_complete(across, 7)
     project(NY - 1)
-    for kind in range(NY - 1):
+    for kind in range(1, NY - 1):
         for way in (0, 1):
             kv_pass(way, 1, kind)
     got(w_sib.at[1], wide(NZ * NY * 16))

time: 73.8 us -> 73.8 us (level)
  no operation moved by 1% of the time
where the time goes in v8:
time: 73.8 us; the launch traced here: 72.9 us
  Pallas kernels  70.9 us (96%)
  local copies, waits for them, and re-layouts  1.98 us (3%)
    pallas_call x1, Pallas kernels, attention(): pl.pallas_call(attention_kernel, out_shape=jax.ShapeDtypeStruct(tokens.sh...  70.9 us
    unnamed x1, local copies, waits for them, and re-layouts  1.98 us

profile of v8, /device:TPU:224, one launch (start us, length us, event | category | flops | bytes accessed | tf_op | source)
XLA Modules:
  0.0 72.9 jit_solution(16801759001685285627)
XLA Ops:
  0.0 70.9 %attention.1 = bf16[160,2048]{1,0:T(8,128)(2,1)} custom-call(bf16[160,2048]{1,0:T(8,128)(2,1)} %tok.1, bf16[32,512]{1,0:T(8,128)(2,1)} %wq.1, bf16[32,512]{1,0:T(8,128)(2,1)} %wk.1, bf16[32,512]{1,0:T(8,128)(2,1)} %wv.1, bf16[32,512]{1,0:T(8,128)(2,1)} %bitcast.2, f32[4]{0:T(128)} %lam.1, f32[1,128]{1,0:T(1,128)} %bitcast.3), custom_call_target="tpu_custom_call" | custom-call | tf_op jit(solution)/shard_map/attention/pallas_call | solution.py:465
  70.9 2.0 %copy.9 = bf16[160,2048]{1,0:T(8,128)(2,1)} copy(bf16[160,2048]{1,0:T(8,128)(2,1)} %attention.1) | data formatting | bytes 1310720
